TPU v7x, 256 devices: a 4x2x16 block of a 4x16x16 slice. The times are simulated.
256 devices in a mesh: grp: 2 (over y), sp: 16 (over z), fs: 4 (over x), tp: 2 (over core).
Axes of the slice: x: 4, y: 2, z: 16, core: 2. Of those that a mesh axis runs over, the one named last changes fastest.
The devices are a block of a 4x16x16 slice.
Arguments:
- tokens: bfloat16 [8, 2048, 2048], P(('grp', 'fs'), 'sp'), parts along dimension 0, may hold values from -6 to 6
- norm_gain: float32 [2048], replicated, may hold values from 0.1 to 1.9
- query_attend: bfloat16 [2048, 8, 128], P(None, ('fs', 'tp')), may hold values from -0.125 to 0.125
- key_attend: bfloat16 [2048, 8, 128], P(None, ('fs', 'tp')), may hold values from -0.125 to 0.125
- value_attend: bfloat16 [2048, 8, 128], P(None, ('fs', 'tp')), may hold values from -0.125 to 0.125
- query_linear: bfloat16 [2048, 8, 128], P(None, ('fs', 'tp')), may hold values from -0.125 to 0.125
- key_linear: bfloat16 [2048, 8, 128], P(None, ('fs', 'tp')), may hold values from -0.125 to 0.125
- value_linear: bfloat16 [2048, 8, 256], P(None, ('fs', 'tp')), may hold values from -0.125 to 0.125
- decay_down: bfloat16 [2048, 32], replicated, may hold values from -0.125 to 0.125
- decay_up: bfloat16 [32, 8, 128], replicated, may hold values from -2.109375 to 2.109375
- decay_bias: float32 [8, 128], replicated, may hold values from -1.5 to 7.5
- log_retain: float32 [8, 2048, 8], P(('grp', 'fs'), 'sp'), parts along dimension 0, may hold values from -1.5 to 0
- query_gain: float32 [64], replicated, may hold values from 0.6 to 4
- key_gain: float32 [8, 2, 64], replicated, may hold values from 0.8 to 14
- diff_lambda: float32 [8], replicated, may hold values from 0.3 to 0.8
- mix_gain: float32 [128], replicated, may hold values from 0.1 to 1.9
- state_gain: float32 [256], replicated, may hold values from 0.1 to 1.9
- init_state: float32 [8, 8, 128, 256], P('grp', ('fs', 'tp')), parts along dimension 0, may hold values from -160 to 160
- output_attend: bfloat16 [1024, 2048], P(None, 'tp'), may hold values from -0.109375 to 0.109375
- output_linear: bfloat16 [2048, 2048], P(None, 'tp'), may hold values from -0.109375 to 0.109375
Outputs:
- mixed_out: bfloat16 [8, 2048, 2048], P(('grp', 'fs'), 'sp', 'tp'), parts along dimension 0
There are 2 independent parts, one for each index of `grp`. A program takes and returns all parts, laid end to end along the dimension named above; an argument that names none is the same for every part. Nothing has to cross between parts.
All inputs are finite; a program needn't handle non-finite values.
Results may differ from a plain program's by a relative error of at most 0.018.
The roundings to bfloat16 on the way count: a program that leaves them out, or rounds other values in their place, can miss the bound.
Values may be sent and summed in bfloat16 or wider, within the bound.
A program may use at most 128 MiB of HBM per device.

v0:
```python
import jax
import jax.numpy as jnp
from jax import lax
from jax.sharding import PartitionSpec as P

MIXER_HEADS = 8
HD_A = 64
DV_A = 128
HDK = 128
HDV = 256
BLK = 64


norm_eps = 1e-06
decay_tau = 16.0


def in_order(tiles, dim):
    tiles = jnp.moveaxis(tiles, 0, dim)
    dims = tiles.shape
    return tiles.reshape(*dims[:dim], dims[dim] * dims[dim + 1], *dims[dim + 2 :])


def sent_to_all(x, axis):
    copies = jnp.broadcast_to(x, (lax.axis_size(axis), *x.shape))
    return lax.all_to_all(copies, axis, split_axis=0, concat_axis=0, tiled=True)


def gather_directly(x, axis, dim):
    return in_order(sent_to_all(x, axis), dim)


def in_one_piece(arrays, axis, dim, along):
    columns = [a.reshape(*a.shape[:along], -1) for a in arrays]
    both = jnp.concatenate(columns, axis=along)
    result, at, finished = (lax.all_gather(both, axis, axis=dim, tiled=True), 0, [])
    for a, column in zip(arrays, columns):
        section = result[..., at : at + column.shape[along]]
        finished.append(section.reshape(*section.shape[:along], *a.shape[along:]))
        at += column.shape[along]
    return tuple(finished)


def entering(part, axis, combine, identity):
    place = lax.axis_index(axis)
    gathered = jax.tree.map(lambda a: lax.all_gather(a, axis), part)
    state = jax.tree.map(lambda a, e: jnp.zeros_like(a) + jnp.asarray(e, a.dtype), part, identity)

    def one(hop, state):
        return combine(
            state, jax.tree.map(lambda a: lax.dynamic_index_in_dim(a, hop, 0, False), gathered)
        )

    return lax.fori_loop(0, place, one, state)


def in_one_piece_2(arrays, axis, dim, along):
    ends, at = ([], 0)
    for a in arrays[:-1]:
        at += a.shape[along]
        ends.append(at)
    both = jnp.concatenate(arrays, axis=along)
    return tuple(jnp.split(lax.all_gather(both, axis, axis=dim, tiled=True), ends, axis=along))


def rms_scale(values, gain):
    widened = values.astype(jnp.float32)
    return (
        widened * lax.rsqrt(jnp.mean(widened * widened, axis=-1, keepdims=True) + norm_eps) * gain
    )


def head_order(fs_size, tp_size, tp_rank):
    per_device = MIXER_HEADS // (fs_size * tp_size)
    owners = jnp.arange(fs_size, dtype=jnp.int32)[:, None] * tp_size + tp_rank
    return (owners * per_device + jnp.arange(per_device, dtype=jnp.int32)[None, :]).reshape(-1)


def linear_blocks(queries, keys_in, values_in, log_decay):
    tok_rows, head_count, key_dim = queries.shape
    value_dim = values_in.shape[-1]
    block_count = tok_rows // BLK

    def split_blocks(source):
        return source.reshape(block_count, BLK, head_count, source.shape[-1])

    causal = (
        jnp.arange(BLK, dtype=jnp.int32)[:, None] >= jnp.arange(BLK, dtype=jnp.int32)[None, :]
    )[None]

    def advance(carry, inputs_now):
        recurrent_state, offset = carry
        question_patch_lines, block_k, value_tile_width, block_log = inputs_now
        running_state = jnp.cumsum(block_log, axis=0)
        pivot = running_state[BLK // 2]
        q_scaled = question_patch_lines * jnp.exp(running_state - pivot[None])
        k_scaled = block_k * jnp.exp(pivot[None] - running_state)
        scores = jnp.einsum("thk,shk->hts", q_scaled, k_scaled)
        scores = jnp.where(causal, scores, 0.0)
        inside_block = jnp.einsum("hts,shv->thv", scores, value_tile_width)
        inside_block = inside_block + jnp.einsum(
            "jwo,wos->jws", question_patch_lines * jnp.exp(running_state), recurrent_state
        )
        final_state = running_state[-1]
        faded_memory_matrix = block_k * jnp.exp(final_state[None] - running_state)
        recurrent_state = recurrent_state * jnp.exp(final_state)[:, :, None] + jnp.einsum(
            "zcb,zcw->cbw", faded_memory_matrix, value_tile_width
        )
        reaching_keys = question_patch_lines * jnp.exp(offset[None] + running_state)
        return ((recurrent_state, offset + final_state), (inside_block, reaching_keys))

    start_carry = (
        jnp.zeros((head_count, key_dim, value_dim), jnp.float32),
        jnp.zeros((head_count, key_dim), jnp.float32),
    )
    (recurrent_state, total_decay), (inside_block, reaching_keys) = lax.scan(
        advance,
        start_carry,
        (
            split_blocks(queries),
            split_blocks(keys_in),
            split_blocks(values_in),
            split_blocks(log_decay),
        ),
    )
    return (
        recurrent_state,
        total_decay,
        inside_block.reshape(tok_rows, head_count, value_dim),
        reaching_keys.reshape(tok_rows, head_count, key_dim),
    )


def body(
    tokens,
    norm_gain,
    query_attend,
    key_attend,
    value_attend,
    query_linear,
    key_linear,
    value_linear,
    decay_down,
    decay_up,
    decay_bias,
    log_retain,
    query_gain,
    key_gain,
    diff_lambda,
    mix_gain,
    state_gain,
    init_state,
    output_attend,
    output_linear,
):
    fs_size = lax.axis_size("fs")
    tp_size = lax.axis_size("tp")
    tp_rank = lax.axis_index("tp")
    tok_rows = tokens.shape[1]
    normed = rms_scale(tokens, norm_gain).astype(jnp.bfloat16)
    normed_rows = normed[0]
    local_weights = (query_attend, key_attend, value_attend, query_linear, key_linear, value_linear)
    widths = [weight.shape[1] * weight.shape[2] for weight in local_weights]
    packed = jnp.concatenate(
        [weight.reshape(weight.shape[0], -1) for weight in local_weights], axis=1
    )
    computed = jnp.einsum(
        "std,dp->stp", gather_directly(normed, "fs", 0), packed, preferred_element_type=jnp.float32
    ).astype(jnp.bfloat16)
    arrived = lax.all_to_all(computed, "fs", split_axis=0, concat_axis=2, tiled=True).reshape(
        tok_rows, fs_size, -1
    )
    sections = []
    column_at = 0
    for weight, width_now in zip(local_weights, widths):
        section = arrived[:, :, column_at : column_at + width_now]
        sections.append(section)
        column_at = column_at + width_now
    projected = tuple(sections)
    q_pair, k_pair, v_attend, q_lin, k_lin, v_lin = projected
    head_ids = head_order(fs_size, tp_size, tp_rank)
    head_count = head_ids.shape[0]
    q_unit = rms_scale(q_pair.reshape(tok_rows, head_count, 2, HD_A), query_gain).astype(
        jnp.bfloat16
    )
    k_unit = rms_scale(
        k_pair.reshape(tok_rows, head_count, 2, HD_A), jnp.take(key_gain, head_ids, axis=0)
    ).astype(jnp.bfloat16)
    sp_start = lax.axis_index("sp") * tok_rows
    query_block = (sp_start + jnp.arange(tok_rows, dtype=jnp.int32)) // BLK
    score_scale = HD_A ** (-0.5)
    blank_attend = (
        jnp.full((head_count, 2, tok_rows), -jnp.inf, jnp.float32),
        jnp.zeros((head_count, 2, tok_rows), jnp.float32),
        jnp.zeros((head_count, 2, tok_rows, DV_A), jnp.float32),
    )
    carry = blank_attend
    seg_keys, seg_values = in_one_piece((k_unit, v_attend), "sp", 0, 2)
    span = seg_keys.shape[0]
    stride_token_lines = 2 * tok_rows
    step_count = span // stride_token_lines
    key_steps = seg_keys.reshape(step_count, stride_token_lines, head_count, 2, HD_A)
    value_steps = seg_values.reshape(step_count, stride_token_lines, head_count, DV_A)

    def one_step(running_state, inputs_now):
        step_index, key_step, value_step = inputs_now
        key_start = step_index * stride_token_lines

        def compute(current):
            run_max, run_total, run_acc = current
            scores = (
                jnp.einsum("qhmd,khmd->hmqk", q_unit, key_step, preferred_element_type=jnp.float32)
                * score_scale
            )
            key_block = (key_start + jnp.arange(stride_token_lines, dtype=jnp.int32)) // BLK
            allowed = query_block[:, None] >= key_block[None, :]
            scores = jnp.where(allowed, scores, -jnp.inf)
            new_max = jnp.maximum(run_max, jnp.max(scores, axis=-1))
            factor = jnp.exp(run_max - new_max)
            raised = jnp.exp(scores - new_max[..., None])
            run_total = run_total * factor + jnp.sum(raised, axis=-1)
            run_acc = run_acc * factor[..., None] + jnp.einsum(
                "hmqk,khv->hmqv",
                raised.astype(jnp.bfloat16),
                value_step,
                preferred_element_type=jnp.float32,
            )
            return (new_max, run_total, run_acc)

        def unchanged(current):
            return current

        return (lax.cond(key_start <= sp_start, compute, unchanged, running_state), None)

    carry, _ = lax.scan(
        one_step, carry, (jnp.arange(step_count, dtype=jnp.int32), key_steps, value_steps)
    )
    run_max, run_total, run_acc = carry
    lambda_heads = jnp.take(diff_lambda, head_ids, axis=0)
    diff_raw = (
        run_acc[:, 0] / run_total[:, 0, :, None]
        - lambda_heads[:, None, None] * run_acc[:, 1] / run_total[:, 1, :, None]
    )
    attend_out = rms_scale(jnp.transpose(diff_raw, (1, 0, 2)), mix_gain).astype(jnp.bfloat16)
    low_rank = jnp.dot(normed_rows, decay_down, preferred_element_type=jnp.float32).astype(
        jnp.bfloat16
    )
    up_columns = jnp.take(decay_up, head_ids, axis=1)
    pre_act = jnp.einsum(
        "tr,rhk->thk", low_rank, up_columns, preferred_element_type=jnp.float32
    ) + jnp.take(decay_bias, head_ids, axis=0)
    retain_heads = jnp.take(log_retain[0], head_ids, axis=1)
    log_decay = jax.nn.log_sigmoid(pre_act) / decay_tau + retain_heads[:, :, None]
    local_state, local_decay, inside_block, reaching_keys = linear_blocks(
        q_lin.astype(jnp.float32) * HDK ** (-0.5),
        k_lin.astype(jnp.float32),
        v_lin.astype(jnp.float32),
        log_decay,
    )

    def chain(earlier, later):
        return (earlier[0] + later[0], earlier[1] * jnp.exp(later[0])[:, :, None] + later[1])

    zero_chain = (jnp.zeros_like(local_decay), jnp.zeros_like(local_state))
    prior_decay, prior_state = entering((local_decay, local_state), "sp", chain, zero_chain)
    start_state = lax.all_to_all(init_state, "fs", split_axis=0, concat_axis=1, tiled=True)[0]
    incoming_state = start_state * jnp.exp(prior_decay)[:, :, None] + prior_state
    linear_raw = inside_block + jnp.einsum("jwo,wos->jws", reaching_keys, incoming_state)
    linear_out = rms_scale(linear_raw, state_gain).astype(jnp.bfloat16)
    out_cols = output_attend.shape[1]
    per_device = MIXER_HEADS // (fs_size * tp_size)
    attend_view = output_attend.reshape(fs_size, tp_size, per_device * DV_A, out_cols)
    linear_view = output_linear.reshape(fs_size, tp_size, per_device * HDV, out_cols)
    blank_out = jnp.zeros((tok_rows, out_cols), jnp.float32)
    running_out = blank_out
    seg_attend, seg_linear = in_one_piece_2((attend_out, linear_out), "tp", 1, 2)
    shard_count = seg_attend.shape[1] // head_count
    first_rank = jnp.int32(0) // head_count
    for shard_step in range(shard_count):
        owner_rank = first_rank + shard_step
        rows_attend = lax.dynamic_index_in_dim(attend_view, owner_rank, 1, keepdims=False).reshape(
            -1, out_cols
        )
        rows_linear = lax.dynamic_index_in_dim(linear_view, owner_rank, 1, keepdims=False).reshape(
            -1, out_cols
        )
        part_attend = seg_attend[
            :, shard_step * head_count : (shard_step + 1) * head_count
        ].reshape(tok_rows, -1)
        part_linear = seg_linear[
            :, shard_step * head_count : (shard_step + 1) * head_count
        ].reshape(tok_rows, -1)
        running_out = running_out + jnp.dot(
            part_attend, rows_attend, preferred_element_type=jnp.float32
        )
        running_out = running_out + jnp.dot(
            part_linear, rows_linear, preferred_element_type=jnp.float32
        )
    return running_out.astype(jnp.bfloat16).reshape(1, tok_rows, out_cols)


def solution(mesh):
    in_specs = (
        P(("grp", "fs"), "sp", None),
        P(),
        P(None, ("fs", "tp"), None),
        P(None, ("fs", "tp"), None),
        P(None, ("fs", "tp"), None),
        P(None, ("fs", "tp"), None),
        P(None, ("fs", "tp"), None),
        P(None, ("fs", "tp"), None),
        P(),
        P(),
        P(),
        P(("grp", "fs"), "sp", None),
        P(),
        P(),
        P(),
        P(),
        P(),
        P("grp", ("fs", "tp"), None, None),
        P(None, "tp"),
        P(None, "tp"),
    )
    out_specs = P(("grp", "fs"), "sp", "tp")
    return jax.shard_map(body, mesh=mesh, in_specs=in_specs, out_specs=out_specs, check_vma=False)
```

profile of v0, /device:TPU:45, one launch (start us, length us, event | category | flops | bytes accessed | tf_op | source)
XLA Modules:
  0.0 280.6 jit_solution(16314881879347051118)
XLA Ops:
  6.6 1.3 fusion.60
  7.8 1.2 fusion.63
  9.1 1.6 broadcast_in_dim.116
  10.7 4.6 %all-to-all-start = ((bf16[4,1,128,2048]{3,2,1,0:T(8,128)(2,1)}), bf16[4,1,128,2048]{3,2,1,0:T(8,128)(2,1)}, u32[]{:S(2)}, u32[]{:S(2)}) async-start(bf16[4,1,128,2048]{3,2,1,0:T(8,128)(2,1)} %broadcast_in_dim.116), calls=%async_computation | async-start | bytes 4194304 | tf_op jit(solution)/shard_map/all_to_all | solution.py:26
  15.4 0.9 bitcast_dynamic-update-slice_fusion.5
  16.3 0.9 bitcast_dynamic-update-slice_fusion.4
  17.2 0.9 bitcast_dynamic-update-slice_fusion.3
  18.1 0.9 bitcast_dynamic-update-slice_fusion.2
  19.0 0.9 bitcast_dynamic-update-slice_fusion.1
  19.9 1.1 bitcast_dynamic-update-slice_fusion
  21.0 17.5 %all-to-all-done = bf16[4,1,128,2048]{3,2,1,0:T(8,128)(2,1)} async-done(((bf16[4,1,128,2048]{3,2,1,0:T(8,128)(2,1)}), bf16[4,1,128,2048]{3,2,1,0:T(8,128)(2,1)}, u32[]{:S(2)}, u32[]{:S(2)}) %all-to-all-start) | async-done | bytes 2097184 | tf_op jit(solution)/shard_map/all_to_all | solution.py:26
  38.5 6.0 %fusion.49 = bf16[4,128,896]{2,1,0:T(8,128)(2,1)} fusion(bf16[2048,896]{1,0:T(8,128)(2,1)} %bitcast_dynamic-update-slice_fusion, bf16[4,1,128,2048]{3,2,1,0:T(8,128)(2,1)} %all-to-all-done), kind=kOutput, calls=%fused_computation.87 | convolution fusion | flops 1879506944 | bytes 6684672 | tf_op jit(solution)/shard_map/std,dp->stp/dot_general | solution.py:167
  44.5 6.3 %all-to-all-start.1 = ((bf16[4,128,896]{2,1,0:T(8,128)(2,1)}), bf16[4,128,896]{2,1,0:T(8,128)(2,1)S(1)}, u32[]{:S(2)}, u32[]{:S(2)}) async-start(bf16[4,128,896]{2,1,0:T(8,128)(2,1)} %fusion.49), calls=%async_computation.1 | async-start | bytes 1835008 | tf_op jit(solution)/shard_map/all_to_all | solution.py:170
  52.7 7.7 %all-to-all-done.1 = bf16[4,128,896]{2,1,0:T(8,128)(2,1)S(1)} async-done(((bf16[4,128,896]{2,1,0:T(8,128)(2,1)}), bf16[4,128,896]{2,1,0:T(8,128)(2,1)S(1)}, u32[]{:S(2)}, u32[]{:S(2)}) %all-to-all-start.1) | async-done | bytes 917536 | tf_op jit(solution)/shard_map/all_to_all | solution.py:170
  60.9 0.7 pad_maximum_fusion.1
  61.8 0.7 gather_fusion.2
  62.7 0.7 fusion.70
  63.4 4.3 %while.46 = (s32[]{:T(128)}, f32[4,128,256]{2,1,0:T(8,128)S(1)}, f32[4,128]{1,0:T(4,128)S(1)}, f32[2,64,4,256]{3,1,0,2:T(8,128)}, bf16[2,64,4,128]{3,2,1,0:T(4,1...) while((s32[]{:T(128)}, f32[4,128,256]{2,1,0:T(8,128)S(1)}, ...), condition=%wide.region_12.13_spmd.clone, body=%wide.region_10.12_spmd.clone.sunk | while | flops 49239040 | bytes 5020301 | solution.py:116
  64.2 0.9 fusion.123
  66.3 0.9 fusion.123
  67.7 0.8 copy-done.4
  68.6 6.7 %all-to-all-start.2 = ((f32[4,1,128,256]{3,2,1,0:T(8,128)}), f32[4,1,128,256]{3,2,1,0:T(8,128)}, u32[]{:S(2)}, u32[]{:S(2)}) async-start(f32[4,1,128,256]{3,2,1,0:T(8,128)} %param.45), calls=%async_computation.2 | async-start | bytes 1048576 | tf_op jit(solution)/shard_map/all_to_all | solution.py:266
  76.0 3.0 %fusion.84 = (bf16[4,1,128,1024]{3,2,1,0:T(8,128)(2,1)S(1)}, bf16[4,1,128,1024]{3,2,1,0:T(8,128)(2,1)}) fusion(bf16[4,2,128,1024]{3,2,1,0:T(8,128)(2,1)} %bitcast.243), kind=kLoop, calls=%fused_computation.160 | loop fusion | bytes 4194304 | tf_op jit(solution)/shard_map/jit(dynamic_index_in_dim)/dynamic_slice | solution.py:281
  78.9 2.4 fusion.82
  81.5 1.0 copy.104
  82.5 43.5 %all-gather.2 = f32[16,4,128]{2,1,0:T(4,128)S(1)} all-gather(f32[1,4,128]{2,1,0:T(4,128)S(1)} %bitcast.259), channel_id=2, replica_groups=mesh['grp'=2,'sp'=16,'fs'=4,'tp'=2] {'sp'}, dimensions={0}, use_global_device_ids=true | all-gather | bytes 34816 | tf_op jit(solution)/shard_map/all_gather | solution.py:46
  126.2 18.6 %all-gather.6.cloned.1.call-done = bf16[2048,4,256]{2,0,1:T(8,128)(2,1)} async-done(((bf16[128,4,256]{2,0,1:T(8,128)(2,1)}), bf16[2048,4,256]{2,0,1:T(8,128)(2,1)}) %all-gather.6.cloned.1.call-update) | async-done | bytes 4194320 | tf_op jit(solution)/shard_map/all_gather | solution.py:36
  144.8 3.9 %fusion.83 = (bf16[2048,4,128]{2,0,1:T(8,128)(2,1)}, bf16[2048,4,128]{2,0,1:T(8,128)(2,1)S(1)}) fusion(bf16[2048,4,256]{2,0,1:T(8,128)(2,1)} %all-gather.6.cloned.1.call-done), kind=kLoop, calls=%fused_computation.159 | loop fusion | bytes 8388608 | tf_op jit(solution)/shard_map/slice | solution.py:38
  148.6 3.3 %reshape.370 = bf16[8,256,4,2,64]{4,3,1,0,2:T(2,128)(2,1)} reshape(bf16[2048,4,128]{2,0,1:T(8,128)(2,1)S(1)} %get-tuple-element.517) | data formatting | bytes 4194304 | tf_op jit(solution)/shard_map/reshape;reshape | solution.py:202
  151.9 10.6 %copy.92 = bf16[8,256,4,2,64]{1,4,3,2,0:T(8,128)(2,1)} copy(bf16[8,256,4,2,64]{4,3,1,0,2:T(2,128)(2,1)} %reshape.370) | data formatting | bytes 4194304
  162.5 1.5 copy.93
  164.1 13.8 %while.47 = (s32[]{:T(128)}, f32[4,2,128]{2,1,0:T(2,128)S(1)}, f32[4,2,128]{2,1,0:T(2,128)S(1)}, f32[4,2,128,128]{3,2,1,0:T(8,128)S(1)}, s32[8]{0:T(128)S(1)}, /...) while((s32[]{:T(128)}, f32[4,2,128]{2,1,0:T(2,128)S(1)}, ...), condition=%wide.region_8.9_spmd.clone.clone, body=%wide.region_3.8_spmd.clone.clone.sunk | while | flops 102802176 | bytes 4990571 | solution.py:235
  165.4 3.1 %conditional.4 = ((f32[4,2,128]{2,1,0:T(2,128)S(1)}, f32[4,2,128]{2,1,0:T(2,128)S(1)}, f32[4,2,128,128]{3,2,1,0:T(8,128)S(1)})) conditional(s32[]{:T(128)} %convert_element_type.111, (f32[4,2,128]{2,1,0:T(2,128)S(1)}, f32[4,2,128]{2,1,0:T(2,128)S(1)}, f32[4,2,128,128]{3,2,1,0:T(8,128)S(1)}) %tuple.121, (s32[128]{0:T(128)S(1)}, s32[]{:T(128)}, ...), branch_computations={%region_4.4_spmd, %region_5.7_spmd.clone} | conditional | flops 102800384 | bytes 4988072 | solution.py:233
  165.6 1.3 fusion.81
  167.1 1.4 convolution_add_fusion.1
  178.3 77.6 %all-gather.8.cloned.1.call-done = f32[64,128,256]{2,1,0:T(8,128)} async-done(((f32[4,128,256]{2,1,0:T(8,128)}), f32[64,128,256]{2,1,0:T(8,128)}) %all-gather.8.cloned.1.call-update) | async-done | bytes 8388624 | tf_op jit(solution)/shard_map/all_gather | solution.py:46
  256.1 1.0 copy-done.9
  257.1 1.4 multiply_reduce_fusion
  258.7 0.9 copy.105
  259.6 3.1 %all_gather.23 = bf16[128,8,384]{2,0,1:T(8,128)(2,1)S(1)} all-gather(bf16[128,4,384]{2,0,1:T(8,128)(2,1)} %copy.105), channel_id=1, replica_groups=mesh['grp'=2,'sp'=16,'fs'=4,'tp'=2] {'tp'}, dimensions={1}, use_global_device_ids=true | all-gather | bytes 1179648 | tf_op jit(solution)/shard_map/all_gather | solution.py:63
  262.7 0.7 fusion.86
  263.5 0.7 fusion.85
  264.2 1.8 copy.122
  265.9 1.7 copy.121
  267.6 0.8 copy.124
  268.6 2.2 fusion.88
  270.9 1.5 fusion.89
  272.7 1.0 fusion.57
  (177 shorter events, 12.5 us)
Async XLA Ops:
  6.5 56.1 %copy-start = (bf16[2048,32]{0,1:T(8,128)(2,1)S(1)}, bf16[2048,32]{0,1:T(8,128)(2,1)}, u32[]{:S(2)}) copy-start(bf16[2048,32]{0,1:T(8,128)(2,1)} %param.36) | copy-start | bytes 393220
  9.1 6.3 %copy-start.13 = (bf16[2048,1,128]{2,0,1:T(8,128)(2,1)S(1)}, bf16[2048,1,128]{2,0,1:T(8,128)(2,1)}, u32[]{:S(2)}) copy-start(bf16[2048,1,128]{2,0,1:T(8,128)(2,1)} %param.30) | copy-start | bytes 1572868
  9.1 7.2 %copy-start.14 = (bf16[2048,1,128]{2,0,1:T(8,128)(2,1)S(1)}, bf16[2048,1,128]{2,0,1:T(8,128)(2,1)}, u32[]{:S(2)}) copy-start(bf16[2048,1,128]{2,0,1:T(8,128)(2,1)} %param.31) | copy-start | bytes 1572868
  10.7 6.5 %copy-start.15 = (bf16[2048,1,128]{2,0,1:T(8,128)(2,1)S(1)}, bf16[2048,1,128]{2,0,1:T(8,128)(2,1)}, u32[]{:S(2)}) copy-start(bf16[2048,1,128]{2,0,1:T(8,128)(2,1)} %param.32) | copy-start | bytes 1572868
  10.7 7.4 %copy-start.16 = (bf16[2048,1,128]{2,0,1:T(8,128)(2,1)S(1)}, bf16[2048,1,128]{2,0,1:T(8,128)(2,1)}, u32[]{:S(2)}) copy-start(bf16[2048,1,128]{2,0,1:T(8,128)(2,1)} %param.33) | copy-start | bytes 1572868
  10.7 27.8 %all-to-all-start = ((bf16[4,1,128,2048]{3,2,1,0:T(8,128)(2,1)}), bf16[4,1,128,2048]{3,2,1,0:T(8,128)(2,1)}, u32[]{:S(2)}, u32[]{:S(2)}) async-start(bf16[4,1,128,2048]{3,2,1,0:T(8,128)(2,1)} %broadcast_in_dim.116), calls=%async_computation | async-start | bytes 4194304 | tf_op jit(solution)/shard_map/all_to_all | solution.py:26
  15.4 3.6 %copy-start.17 = (bf16[2048,1,128]{2,0,1:T(8,128)(2,1)S(1)}, bf16[2048,1,128]{2,0,1:T(8,128)(2,1)}, u32[]{:S(2)}) copy-start(bf16[2048,1,128]{2,0,1:T(8,128)(2,1)} %param.34) | copy-start | bytes 1572868
  15.4 4.5 %copy-start.11 = (bf16[2048,1,256]{2,0,1:T(8,128)(2,1)S(1)}, bf16[2048,1,256]{2,0,1:T(8,128)(2,1)}, u32[]{:S(2)}) copy-start(bf16[2048,1,256]{2,0,1:T(8,128)(2,1)} %param.35) | copy-start | bytes 3145732
  20.9 29.8 %copy-start.22 = (f32[8,2,64]{2,1,0:T(2,128)S(1)}, f32[8,2,64]{2,1,0:T(2,128)}, u32[]{:S(2)}) copy-start(f32[8,2,64]{2,1,0:T(2,128)} %param.41) | copy-start | bytes 12292
  21.0 30.5 %copy-start.21 = (f32[8,128]{1,0:T(8,128)S(1)}, f32[8,128]{1,0:T(8,128)}, u32[]{:S(2)}) copy-start(f32[8,128]{1,0:T(8,128)} %param.38) | copy-start | bytes 12292
  21.0 31.1 %copy-start.3 = (f32[1,128,8]{1,2,0:T(8,128)S(1)}, f32[1,128,8]{1,2,0:T(8,128)}, u32[]{:S(2)}) copy-start(f32[1,128,8]{1,2,0:T(8,128)} %param.39) | copy-start | bytes 12292
  44.4 17.4 %copy-start.10 = (bf16[32,8,128]{2,1,0:T(8,128)(2,1)S(1)}, bf16[32,8,128]{2,1,0:T(8,128)(2,1)}, u32[]{:S(2)}) copy-start(bf16[32,8,128]{2,1,0:T(8,128)(2,1)} %param.37) | copy-start | bytes 196612
  44.5 16.0 %all-to-all-start.1 = ((bf16[4,128,896]{2,1,0:T(8,128)(2,1)}), bf16[4,128,896]{2,1,0:T(8,128)(2,1)S(1)}, u32[]{:S(2)}, u32[]{:S(2)}) async-start(bf16[4,128,896]{2,1,0:T(8,128)(2,1)} %fusion.49), calls=%async_computation.1 | async-start | bytes 1835008 | tf_op jit(solution)/shard_map/all_to_all | solution.py:170
  50.8 94.0 %all-gather.6.cloned.1.call-start = ((), (), s32[]{:S(2)}) async-start(), calls=%async_computation.3 | async-start | bytes 4456448 | tf_op jit(solution)/shard_map/all_gather | solution.py:36
  61.7 194.2 %all-gather.8.cloned.1.call-start = ((), (), s32[]{:S(2)}) async-start(), calls=%async_computation.4 | async-start | bytes 8912896 | tf_op jit(solution)/shard_map/all_gather | solution.py:46
  63.4 11.9 %copy-start.2 = (f32[8]{0:T(128)S(1)}, f32[8]{0:T(128)}, u32[]{:S(2)}) copy-start(f32[8]{0:T(128)} %param.42) | copy-start | bytes 100
  67.7 0.8 copy-start.4
  67.7 8.3 %copy-start.19 = (bf16[2,64,4,128]{3,2,1,0:T(4,128)(2,1)}, bf16[2,64,4,128]{3,2,1,0:T(4,128)(2,1)S(1)}, u32[]{:S(2)}) copy-start(bf16[2,64,4,128]{3,2,1,0:T(4,128)(2,1)S(1)} %get-tuple-element.237) | copy-start | bytes 393220
  68.6 187.5 %all-to-all-start.2 = ((f32[4,1,128,256]{3,2,1,0:T(8,128)}), f32[4,1,128,256]{3,2,1,0:T(8,128)}, u32[]{:S(2)}, u32[]{:S(2)}) async-start(f32[4,1,128,256]{3,2,1,0:T(8,128)} %param.45), calls=%async_computation.2 | async-start | bytes 1048576 | tf_op jit(solution)/shard_map/all_to_all | solution.py:266
  75.9 3.0 %copy-start.7 = (bf16[2048,1024]{1,0:T(8,128)(2,1)S(1)}, bf16[2048,1024]{1,0:T(8,128)(2,1)}, u32[]{:S(2)}) copy-start(bf16[2048,1024]{1,0:T(8,128)(2,1)} %param.47) | copy-start | bytes 12582916
  78.9 2.5 copy-start.18
  78.9 47.1 %copy-start.24 = (f32[64]{0:T(128)S(1)}, f32[64]{0:T(128)}, u32[]{:S(2)}) copy-start(f32[64]{0:T(128)} %param.40) | copy-start | bytes 772
  151.9 10.6 %copy-start.6 = (bf16[2048,4,128]{2,0,1:T(8,128)(2,1)S(1)}, bf16[2048,4,128]{2,0,1:T(8,128)(2,1)}, u32[]{:S(2)}) copy-start(bf16[2048,4,128]{2,0,1:T(8,128)(2,1)} %get-tuple-element.516) | copy-start | bytes 6291460
  164.1 14.1 %copy-start.25 = (f32[128]{0:T(128)S(1)}, f32[128]{0:T(128)}, u32[]{:S(2)}) copy-start(f32[128]{0:T(128)} %param.43) | copy-start | bytes 1540
  256.0 1.0 copy-start.9
  256.0 1.1 copy-start.20
  256.0 2.5 copy-start.23
  259.6 11.2 %copy-start.5 = (bf16[4,1,256,1024]{3,2,1,0:T(8,128)(2,1)S(1)}, bf16[4,1,256,1024]{3,2,1,0:T(8,128)(2,1)}, u32[]{:S(2)}) copy-start(bf16[4,1,256,1024]{3,2,1,0:T(8,128)(2,1)} %get-tuple-element.515) | copy-start | bytes 6291460
  268.5 3.9 %copy-start.12 = (bf16[128,4,128]{0,2,1:T(8,128)(2,1)S(1)}, bf16[128,4,128]{0,2,1:T(8,128)(2,1)}, u32[]{:S(2)}) copy-start(bf16[128,4,128]{0,2,1:T(8,128)(2,1)} %copy.121) | copy-start | bytes 393220
  268.6 3.7 %copy-start.8 = (bf16[4,1,128,1024]{3,2,1,0:T(8,128)(2,1)S(1)}, bf16[4,1,128,1024]{3,2,1,0:T(8,128)(2,1)}, u32[]{:S(2)}) copy-start(bf16[4,1,128,1024]{3,2,1,0:T(8,128)(2,1)} %get-tuple-element.519) | copy-start | bytes 3145732
  270.8 2.9 %copy-start.1 = (bf16[2048,32]{0,1:T(8,128)(2,1)S(1)}, bf16[2048,32]{0,1:T(8,128)(2,1)}, u32[]{:S(2)}) copy-start(bf16[2048,32]{0,1:T(8,128)(2,1)} %param.36) | copy-start | bytes 393220
Sparse Core Ops, SparseCore 0:
  61.8 82.8 all-gather.5
  146.6 109.3 all-gather.7
where the time goes:
time: 284 us; the launch traced here: 281 us
  waiting for transfers between devices  122 us (43%)
  local copies, waits for them, and re-layouts  50.1 us (18%)
  blocking collectives  46.6 us (16%)
  matrix products  18.8 us (7%)
  starting transfers between devices  17.8 us (6%)
  between operations  14 us (5%)
  loops' own time  5.99 us (2%)
  other arithmetic  5.69 us (2%)
    all_gather x1, waiting for transfers between devices, entering(): gathered = jax.tree.map(lambda a: lax.all_gather(a, axis), part)  77.6 us
    all_gather x1, blocking collectives, entering(): gathered = jax.tree.map(lambda a: lax.all_gather(a, axis), part)  43.5 us
    unnamed x63, local copies, waits for them, and re-layouts  22.9 us
    all_gather x1, waiting for transfers between devices, in_one_piece(): lax.all_gather(both, axis, axis=dim, tiled=True)  18.6 us
    all_to_all x1, waiting for transfers between devices, sent_to_all(): return lax.all_to_all(copies, axis, split_axis=0, concat_axis=0, tiled=True)  17.5 us
    all_to_all x1, waiting for transfers between devices, body(): lax.all_to_all(computed, 'fs', split_axis=0, concat_axis=2, tiled=True)  7.74 us
    all_to_all x1, starting transfers between devices, body(): lax.all_to_all(init_state, 'fs', split_axis=0, concat_axis=1, tiled=True)[0]  6.75 us
    all_to_all x1, starting transfers between devices, body(): lax.all_to_all(computed, 'fs', split_axis=0, concat_axis=2, tiled=True)  6.31 us
  transfers between devices with their start and end apart: 5, of which 4 were waited for; matrix products, arithmetic and copies ran while one was open for 17% of the time, Pallas kernels for 0%

commit v1 on v0

v1 whole, which is shorter than its diff:
```python
import functools

import jax
import jax.numpy as jnp
from jax import lax
from jax.experimental import pallas as pl
from jax.experimental.pallas import tpu as pltpu
from jax.sharding import PartitionSpec as P

HEADS = 8
HALF = 64
HD = 128
HV = 256
BLK = 64
RANK = 32
EPS = 1e-06
TAU = 16.0
MESH = pl.DeviceIdType.MESH
F32 = jnp.float32
BF16 = jnp.bfloat16
NT = (((1,), (1,)), ((), ()))
TN = (((0,), (0,)), ((), ()))
CHAIN_FIRST_UP_TO = 8


def dot(a, b, dims=(((1,), (0,)), ((), ())), **kw):
    return lax.dot_general(a, b, dims, preferred_element_type=F32, **kw)


def iota(shape, dim):
    return lax.broadcasted_iota(jnp.int32, shape, dim)


def turned(row, n):
    return jnp.transpose(jnp.broadcast_to(row, (n, row.shape[-1])))


def unit_norm(x, gain):
    left = iota(x.shape, 1) < HALF
    sq = x * x
    a = jnp.sum(jnp.where(left, sq, 0.0), axis=1, keepdims=True)
    b = jnp.sum(jnp.where(left, 0.0, sq), axis=1, keepdims=True)
    mean = jnp.where(left, a, b) * (1.0 / HALF)
    return (x * lax.rsqrt(mean + EPS) * gain).astype(BF16)


def project_kernel(
    tok_ref,
    gain_ref,
    wqa,
    wka,
    wva,
    wql,
    wkl,
    wvl,
    down_ref,
    up_ref,
    bias_ref,
    retain_ref,
    qgain_ref,
    kgain_ref,
    kv_out,
    q_out,
    qr_out,
    inside_out,
    local_out,
    decay_out,
    weights,
    gath,
    rets,
    w_sem,
    send,
    recv,
    r_send,
    r_recv,
):
    x = lax.axis_index("fs")
    t = lax.axis_index("tp")
    n = lax.axis_size("fs")
    right, left, far = lax.rem(x + 1, n), lax.rem(x + n - 1, n), lax.rem(x + 2, n)
    head = x * 2 + t
    rows = tok_ref.shape[0]

    copies = []
    at = 0
    for i, w in enumerate((wqa, wka, wva, wql, wkl, wvl)):
        width = w.shape[1]
        copies.append(
            pltpu.make_async_copy(w, weights.at[:, pl.ds(at, width)], w_sem.at[i])
        )
        at += width
    for c in copies:
        c.start()

    barrier = pltpu.get_barrier_semaphore()
    for peer in (left, right, far):
        pl.semaphore_signal(barrier, inc=1, device_id={"fs": peer}, device_id_type=MESH)
    pl.semaphore_signal(barrier, inc=1, device_id={"tp": 1 - t}, device_id_type=MESH)

    gain = gain_ref[...]

    def normalize(start):
        part = tok_ref[pl.ds(start, 32), :].astype(F32)
        mean = jnp.mean(part * part, axis=1, keepdims=True)
        gath[0, pl.ds(start, 32), :] = (part * lax.rsqrt(mean + EPS) * gain).astype(BF16)

    lo = pl.multiple_of(t * 64, 64)
    hi = pl.multiple_of(t * 64 + 32, 32)
    other = pl.multiple_of((1 - t) * 64, 64)
    other_hi = pl.multiple_of((1 - t) * 64 + 32, 32)
    rets[0] = retain_ref[...]
    normalize(lo)
    normalize(hi)
    pl.semaphore_wait(barrier, 4)

    def remote(i, slot_from, slot_to, start, peer):
        return pltpu.make_async_remote_copy(
            src_ref=gath.at[slot_from, pl.ds(start, 32), :],
            dst_ref=gath.at[slot_to, pl.ds(start, 32), :],
            send_sem=send.at[i],
            recv_sem=recv.at[i],
            device_id=peer,
            device_id_type=MESH,
        )

    to_right = {"fs": right}
    to_left = {"fs": left}
    partner = {"tp": 1 - t}
    r0 = remote(0, 0, 1, lo, to_right)
    l1 = remote(1, 0, 3, hi, to_left)
    r1 = remote(2, 0, 1, hi, to_right)
    l0 = remote(3, 0, 3, lo, to_left)
    for c in (r0, l1, r1, l0):
        c.start()
    small = []
    for i, (slot, peer) in enumerate(((1, right), (3, left), (2, far))):
        small.append(
            pltpu.make_async_remote_copy(
                src_ref=rets.at[0],
                dst_ref=rets.at[slot],
                send_sem=r_send.at[i],
                recv_sem=r_recv.at[i],
                device_id={"fs": peer},
                device_id_type=MESH,
            )
        )
    for c in small:
        c.start()
    normalize(other)
    normalize(other_hi)
    for c in copies:
        c.wait()

    up_rows = up_ref[...]
    pick = (iota((RANK, RANK * HEADS), 1) == iota((RANK, RANK * HEADS), 0) * HEADS + head)
    pick = jnp.where(pick, 1.0, 0.0).astype(BF16)
    bias = bias_ref[pl.ds(head, 1), :]
    qg = qgain_ref[...]
    qgain = jnp.concatenate([qg, qg], axis=1)
    kg = kgain_ref[pl.ds(head, 1)][0]
    kgain = jnp.concatenate([kg[0:1], kg[1:2]], axis=1)
    rr, cc = iota((rows, rows), 0), iota((rows, rows), 1)
    same = (rr // BLK) == (cc // BLK)
    tri = jnp.where(same & (rr >= cc), 1.0, 0.0)
    second = iota((rows, HD), 0) >= BLK

    def finish(slot, seq):
        act = gath[slot]
        got = dot(act, weights[...]).astype(BF16)
        low = dot(act, down_ref[...], NT).astype(BF16)
        pre = dot(dot(low, pick).astype(BF16), up_rows) + bias
        log_sig = jnp.minimum(pre, 0.0) - jnp.log1p(jnp.exp(-jnp.abs(pre)))
        keep = jnp.sum(
            jnp.where(iota((HEADS, rows), 0) == head, rets[slot], 0.0), axis=0, keepdims=True
        )
        log_decay = log_sig * (1.0 / TAU) + turned(keep, HD)
        run = dot(tri, log_decay, precision=lax.Precision.HIGHEST)
        q_unit = unit_norm(got[:, 0:HD].astype(F32), qgain)
        k_unit = unit_norm(got[:, HD : 2 * HD].astype(F32), kgain)
        kv_out[seq, :, 0:HD] = k_unit
        kv_out[seq, :, HD : 2 * HD] = got[:, 2 * HD : 3 * HD]
        q_out[seq] = (q_unit.astype(F32) * (HALF**-0.5)).astype(BF16)
        q_lin = got[:, 3 * HD : 4 * HD].astype(F32) * (HD**-0.5)
        k_lin = got[:, 4 * HD : 5 * HD].astype(F32)
        v_lin = got[:, 5 * HD :]
        pivot = jnp.where(second, run[BLK + BLK // 2 : BLK + BLK // 2 + 1], run[BLK // 2 : BLK // 2 + 1])
        end0, end1 = run[BLK - 1 : BLK], run[2 * BLK - 1 : 2 * BLK]
        ends = jnp.where(second, end1, end0)
        scores = dot(
            (q_lin * jnp.exp(run - pivot)).astype(BF16),
            (k_lin * jnp.exp(pivot - run)).astype(BF16),
            NT,
        )
        q_here = q_lin * jnp.exp(run)
        k_left = k_lin * jnp.exp(ends - run)
        across = dot(q_here.astype(BF16), k_left.astype(BF16), NT)
        later = (rr >= BLK) & (cc < BLK)
        mixed = jnp.where(same & (rr >= cc), scores, jnp.where(later, across, 0.0))
        inside_out[seq] = dot(mixed.astype(BF16), v_lin)
        k_out = k_left * jnp.where(second, 1.0, jnp.exp(end1))
        local_out[seq] = dot(k_out.astype(BF16), v_lin, TN)
        qr_out[seq] = (q_here * jnp.where(second, jnp.exp(end0), 1.0)).astype(BF16)
        decay_out[seq] = turned(jnp.exp(end0 + end1), HD)

    finish(0, x)

    f_right = remote(4, 1, 2, lo, to_right)
    f_left = remote(5, 3, 2, hi, to_left)
    relays = {
        "r0": remote(6, 1, 1, lo, partner),
        "l1": remote(7, 3, 3, hi, partner),
        "r1": remote(8, 1, 1, hi, partner),
        "l0": remote(9, 3, 3, lo, partner),
        "f0": remote(10, 2, 2, lo, partner),
        "f1": remote(11, 2, 2, hi, partner),
    }
    r0.wait_recv()
    f_right.start()
    l1.wait_recv()
    f_left.start()
    relays["r0"].start()
    relays["l1"].start()
    r1.wait_recv()
    relays["r1"].start()
    l0.wait_recv()
    relays["l0"].start()
    for c in small:
        c.wait_recv()
    relays["r0"].wait_recv()
    relays["r1"].wait_recv()
    finish(1, left)
    f_right.wait_recv()
    relays["f0"].start()
    f_left.wait_recv()
    relays["f1"].start()
    relays["l1"].wait_recv()
    relays["l0"].wait_recv()
    finish(3, right)
    relays["f0"].wait_recv()
    relays["f1"].wait_recv()
    finish(2, far)
    for c in (r0, l1, r1, l0, f_right, f_left, *relays.values(), *small):
        c.wait_send()


def mix_kernel(
    kv_ref,
    q_ref,
    qr_ref,
    inside_ref,
    local_ref,
    decay_ref,
    init_ref,
    lam_ref,
    mix_gain_ref,
    state_gain_ref,
    wa_hbm,
    wl_hbm,
    out_ref,
    wa,
    wl,
    kvbuf,
    qbuf,
    abuf,
    sin,
    sout,
    lbuf,
    fa,
    fl,
    w_sem,
    kv_send,
    kv_recv,
    q_send,
    q_recv,
    relay_send,
    a_send,
    a_recv,
    c_send,
    c_recv,
    l_send,
    l_recv,
    f_send,
    f_recv,
):
    x = lax.axis_index("fs")
    t = lax.axis_index("tp")
    z = lax.axis_index("sp")
    n_sp = lax.axis_size("sp")
    n_fs = lax.axis_size("fs")
    head = x * 2 + t
    odd = lax.rem(x, 2)
    pair = z // 2
    worker = lax.rem(z, 2) == odd
    w_seq = pair // 2
    w_tp = lax.rem(pair, 2)
    w_head = x * 2 + w_tp
    partner = {"tp": 1 - t}

    def plane(seq, xx, tt):
        return 2 * (2 * seq + tt) + lax.rem(xx, 2)

    load_a = pltpu.make_async_copy(wa_hbm, wa, w_sem.at[0])
    load_l = pltpu.make_async_copy(wl_hbm, wl, w_sem.at[1])
    load_a.start()
    load_l.start()

    barrier = pltpu.get_barrier_semaphore()

    def greet(dev, ok=None):
        def go():
            pl.semaphore_signal(barrier, inc=1, device_id=dev, device_id_type=MESH)

        if ok is None:
            go()
        else:
            pl.when(ok)(go)

    def greet_column(i, c):
        zz = lax.rem(z + i, n_sp)
        greet({"sp": zz})
        greet({"sp": zz, "tp": 1 - t})
        return c

    greet(partner)
    lax.fori_loop(1, n_sp, greet_column, 0)
    for i in range(1, n_fs):
        xx = lax.rem(x + i, n_fs)
        for tt in range(2):
            greet({"fs": xx, "tp": tt})
    for i in range(n_fs):
        xx = lax.rem(x + i, n_fs)
        for tt in range(2):
            pp = plane(x, xx, tt)
            greet({"fs": xx, "sp": pp}, None if i else pp != z)
    expected = 2 * n_sp - 1 + 2 * (n_fs - 1)
    is_worker = worker.astype(jnp.int32)
    expected = expected + is_worker * n_sp - is_worker * (w_seq == x).astype(jnp.int32)
    pl.semaphore_wait(barrier, expected)

    kv_core = lax.rem(z, 2)

    def kv_copy(seq, dst_z, dst_t):
        return pltpu.make_async_remote_copy(
            src_ref=kv_ref.at[seq],
            dst_ref=kvbuf.at[z],
            send_sem=kv_send.at[seq],
            recv_sem=kv_recv.at[z],
            device_id={"sp": dst_z, "tp": dst_t},
            device_id_type=MESH,
        )

    def q_copy(seq, dst_z, dst_t):
        return pltpu.make_async_remote_copy(
            src_ref=q_ref.at[seq, pl.ds(dst_t * HALF, HALF), :],
            dst_ref=qbuf.at[z],
            send_sem=q_send.at[seq, dst_t],
            recv_sem=q_recv.at[z],
            device_id={"sp": dst_z, "tp": dst_t},
            device_id_type=MESH,
        )

    def spread(start):
        for seq in range(4):
            pz = plane(seq, x, t)
            mine = (pz == z) & (kv_core == t)
            c = kv_copy(seq, pz, kv_core)
            pl.when(jnp.logical_not(mine))(c.start if start else c.wait_send)
            if start:

                @pl.when(mine)
                def _():
                    kvbuf[z] = kv_ref[seq]

            for tt in range(2):
                mine_q = (pz == z) & (t == tt)
                c = q_copy(seq, pz, tt)
                pl.when(jnp.logical_not(mine_q))(c.start if start else c.wait_send)
                if start:

                    @pl.when(mine_q)
                    def _():
                        qbuf[z] = q_ref[seq, tt * HALF : (tt + 1) * HALF, :]

    def chain_copy(seq):
        return pltpu.make_async_remote_copy(
            src_ref=sout.at[seq],
            dst_ref=sin.at[seq],
            send_sem=c_send.at[seq],
            recv_sem=c_recv.at[seq],
            device_id={"sp": lax.rem(z + 1, n_sp)},
            device_id_type=MESH,
        )

    def lin_copy(seq, tt):
        return pltpu.make_async_remote_copy(
            src_ref=lbuf.at[seq, pl.ds(tt * HALF, HALF), :],
            dst_ref=fl.at[tt, :, pl.ds(pl.multiple_of(head * HV, HV), HV)],
            send_sem=l_send.at[seq, tt],
            recv_sem=l_recv.at[head],
            device_id={"fs": seq, "tp": tt},
            device_id_type=MESH,
        )

    first, last = z == 0, z == n_sp - 1

    def chain():
        for seq in range(4):

            @pl.when(first)
            def _():
                sin[seq] = init_ref[seq].astype(BF16)
                d = decay_ref[seq]
                d = jnp.concatenate([d, d], axis=1)
                sout[seq] = (init_ref[seq] * d + local_ref[seq]).astype(BF16)
                chain_copy(seq).start()

            @pl.when(jnp.logical_not(first | last))
            def _():
                chain_copy(seq).wait_recv()
                d = decay_ref[seq]
                d = jnp.concatenate([d, d], axis=1)
                sout[seq] = (sin[seq].astype(F32) * d + local_ref[seq]).astype(BF16)
                chain_copy(seq).start()

        for seq in range(4):

            @pl.when(last)
            def _():
                chain_copy(seq).wait_recv()

            raw = inside_ref[seq] + dot(qr_ref[seq], sin[seq])
            mean = jnp.mean(raw * raw, axis=1, keepdims=True)
            lin = (raw * lax.rsqrt(mean + EPS) * state_gain_ref[...]).astype(BF16)
            lbuf[seq] = lin
            for tt in range(2):
                mine = (x == seq) & (t == tt)
                pl.when(jnp.logical_not(mine))(lin_copy(seq, tt).start)

                @pl.when(mine)
                def _():
                    fl[tt, :, pl.ds(pl.multiple_of(head * HV, HV), HV)] = lin[
                        tt * HALF : (tt + 1) * HALF
                    ]

    def relay_copy(j):
        zz = t + 2 * j
        return pltpu.make_async_remote_copy(
            src_ref=kvbuf.at[zz],
            dst_ref=kvbuf.at[zz],
            send_sem=relay_send.at[j],
            recv_sem=kv_recv.at[zz],
            device_id=partner,
            device_id_type=MESH,
        )

    def kv_arrival(zz):
        return pltpu.make_async_remote_copy(
            src_ref=kv_ref.at[0],
            dst_ref=kvbuf.at[zz],
            send_sem=kv_send.at[0],
            recv_sem=kv_recv.at[zz],
            device_id=partner,
            device_id_type=MESH,
        )

    def q_arrival(zz):
        return pltpu.make_async_remote_copy(
            src_ref=q_ref.at[0, pl.ds(0, HALF), :],
            dst_ref=qbuf.at[zz],
            send_sem=q_send.at[0, 0],
            recv_sem=q_recv.at[zz],
            device_id=partner,
            device_id_type=MESH,
        )

    def a_copy(i):
        return pltpu.make_async_remote_copy(
            src_ref=abuf.at[i],
            dst_ref=fa.at[t, :, pl.ds(pl.multiple_of(w_head * HD, HD), HD)],
            send_sem=a_send.at[i],
            recv_sem=a_recv.at[w_head],
            device_id={"fs": w_seq, "sp": i},
            device_id_type=MESH,
        )

    def attend():
        lam = lam_ref[w_head]
        own = t == w_tp
        for g in range(4):
            span = 512 * (g + 1)
            for j in range(2 * g, 2 * g + 2):
                zz = t + 2 * j
                pl.when(jnp.logical_not(own & (zz == z)))(kv_arrival(zz).wait_recv)
                relay_copy(j).start()
            for i in range(4 * g, 4 * g + 4):
                pl.when(jnp.logical_not(own & (z == i)))(q_arrival(i).wait_recv)
            for j in range(2 * g, 2 * g + 2):
                kv_arrival((1 - t) + 2 * j).wait_recv()

            def one(i, c):
                qi = qbuf[i]
                lane = iota((HALF, HD), 1)
                zero = jnp.zeros_like(qi)
                q2 = jnp.concatenate(
                    [jnp.where(lane < HALF, qi, zero), jnp.where(lane < HALF, zero, qi)], axis=0
                )
                n_old = 4 * g
                keys = kvbuf[n_old : n_old + 4, :, 0:HD].reshape(512, HD)
                vals = kvbuf[n_old : n_old + 4, :, HD:].reshape(512, HD)
                s = dot(q2, keys, NT)
                limit = (2 * i + t + 1) * BLK - span + 512
                s = jnp.where(iota(s.shape, 1) < limit, s, -jnp.inf)
                top = jnp.max(s, axis=1, keepdims=True)
                if g:
                    old_keys = kvbuf[0:n_old, :, 0:HD].reshape(span - 512, HD)
                    old_vals = kvbuf[0:n_old, :, HD:].reshape(span - 512, HD)
                    s_old = dot(q2, old_keys, NT)
                    top = jnp.maximum(top, jnp.max(s_old, axis=1, keepdims=True))
                p = jnp.exp(s - top)
                total = jnp.sum(p, axis=1, keepdims=True)
                acc = dot(p.astype(BF16), vals)
                if g:
                    p_old = jnp.exp(s_old - top)
                    total = total + jnp.sum(p_old, axis=1, keepdims=True)
                    acc = acc + dot(p_old.astype(BF16), old_vals)
                acc = acc / total
                diff = acc[:HALF] - lam * acc[HALF:]
                mean = jnp.mean(diff * diff, axis=1, keepdims=True)
                res = (diff * lax.rsqrt(mean + EPS) * mix_gain_ref[...]).astype(BF16)
                abuf[i] = res
                mine = (x == w_seq) & (z == i)
                pl.when(jnp.logical_not(mine))(a_copy(i).start)

                @pl.when(mine)
                def _():
                    fa[t, :, pl.ds(pl.multiple_of(w_head * HD, HD), HD)] = res

                return c

            lax.fori_loop(4 * g, 4 * g + 4, one, 0)

    spread(True)

    early = (z <= CHAIN_FIRST_UP_TO).astype(jnp.int32)

    def phase(i, c):
        is_chain = lax.rem(i + early, 2) == 1
        pl.when(is_chain)(chain)
        pl.when(jnp.logical_not(is_chain) & worker)(attend)
        return c

    lax.fori_loop(0, 2, phase, 0)

    def a_arrival(hh):
        return pltpu.make_async_remote_copy(
            src_ref=abuf.at[0],
            dst_ref=fa.at[t, :, pl.ds(hh * HD, HD)],
            send_sem=a_send.at[0],
            recv_sem=a_recv.at[hh],
            device_id=partner,
            device_id_type=MESH,
        )

    def l_arrival(hh):
        return pltpu.make_async_remote_copy(
            src_ref=lbuf.at[0, pl.ds(0, HALF), :],
            dst_ref=fl.at[t, :, pl.ds(hh * HV, HV)],
            send_sem=l_send.at[0, 0],
            recv_sem=l_recv.at[hh],
            device_id=partner,
            device_id_type=MESH,
        )

    def swap(buf, i):
        return pltpu.make_async_remote_copy(
            src_ref=buf.at[t],
            dst_ref=buf.at[t],
            send_sem=f_send.at[i],
            recv_sem=f_recv.at[i],
            device_id=partner,
            device_id_type=MESH,
        )

    for hh in range(HEADS):
        from_me = (x == hh // 2) & (z == plane(x, hh // 2, hh % 2))
        pl.when(jnp.logical_not(from_me))(a_arrival(hh).wait_recv)
    swap(fa, 0).start()
    load_a.wait()
    load_l.wait()
    swap(fa, 0).wait_recv()
    acc = dot(fa[...].reshape(2 * HALF, HEADS * HD), wa[...])
    for hh in range(HEADS):
        pl.when(head != hh)(l_arrival(hh).wait_recv)
    swap(fl, 1).start()
    swap(fl, 1).wait_recv()
    acc = acc + dot(fl[...].reshape(2 * HALF, HEADS * HV), wl[...])
    out_ref[...] = acc.astype(BF16)

    swap(fa, 0).wait_send()
    swap(fl, 1).wait_send()
    spread(False)
    for seq in range(4):
        pl.when(jnp.logical_not(last))(chain_copy(seq).wait_send)
        for tt in range(2):
            mine = (x == seq) & (t == tt)
            pl.when(jnp.logical_not(mine))(lin_copy(seq, tt).wait_send)

    @pl.when(worker)
    def _():
        for j in range(8):
            relay_copy(j).wait_send()

        def done(i, c):
            mine = (x == w_seq) & (z == i)
            pl.when(jnp.logical_not(mine))(a_copy(i).wait_send)
            return c

        lax.fori_loop(0, n_sp, done, 0)


def body(
    tokens,
    norm_gain,
    query_attend,
    key_attend,
    value_attend,
    query_linear,
    key_linear,
    value_linear,
    decay_down,
    decay_up,
    decay_bias,
    log_retain,
    query_gain,
    key_gain,
    diff_lambda,
    mix_gain,
    state_gain,
    init_state,
    output_attend,
    output_linear,
):
    rows, width = tokens.shape[1:]
    n_fs = lax.axis_size("fs")
    n_sp = lax.axis_size("sp")
    cols = output_attend.shape[1]
    flat = [
        w.reshape(w.shape[0], -1)
        for w in (query_attend, key_attend, value_attend, query_linear, key_linear, value_linear)
    ]
    total = sum(w.shape[1] for w in flat)
    vmem = pl.BlockSpec(memory_space=pltpu.VMEM)
    smem = pl.BlockSpec(memory_space=pltpu.SMEM)
    hbm = pl.BlockSpec(memory_space=pl.ANY)
    dma = pltpu.SemaphoreType.DMA

    made = pl.pallas_call(
        project_kernel,
        out_shape=[
            jax.ShapeDtypeStruct((n_fs, rows, 2 * HD), BF16),
            jax.ShapeDtypeStruct((n_fs, rows, HD), BF16),
            jax.ShapeDtypeStruct((n_fs, rows, HD), BF16),
            jax.ShapeDtypeStruct((n_fs, rows, HV), F32),
            jax.ShapeDtypeStruct((n_fs, HD, HV), F32),
            jax.ShapeDtypeStruct((n_fs, HD, HD), F32),
        ],
        in_specs=[vmem, vmem] + [hbm] * 6 + [vmem] * 6,
        out_specs=[vmem] * 6,
        scratch_shapes=[
            pltpu.VMEM((width, total), BF16),
            pltpu.VMEM((n_fs, rows, width), BF16),
            pltpu.VMEM((n_fs, HEADS, rows), F32),
            dma((6,)),
            dma((12,)),
            dma((12,)),
            dma((3,)),
            dma((3,)),
        ],
        compiler_params=pltpu.CompilerParams(
            collective_id=0, has_side_effects=True, vmem_limit_bytes=40 * 1024 * 1024
        ),
        name="project",
    )(
        tokens[0],
        norm_gain.reshape(1, -1),
        *flat,
        decay_down.T,
        decay_up.reshape(-1, HD),
        decay_bias,
        log_retain[0].T,
        query_gain.reshape(1, -1),
        key_gain,
    )

    out = pl.pallas_call(
        mix_kernel,
        out_shape=jax.ShapeDtypeStruct((rows, cols), BF16),
        in_specs=[vmem] * 6 + [vmem, smem, vmem, vmem, hbm, hbm],
        out_specs=vmem,
        scratch_shapes=[
            pltpu.VMEM(output_attend.shape, BF16),
            pltpu.VMEM(output_linear.shape, BF16),
            pltpu.VMEM((n_sp, rows, 2 * HD), BF16),
            pltpu.VMEM((n_sp, HALF, HD), BF16),
            pltpu.VMEM((n_sp, HALF, HD), BF16),
            pltpu.VMEM((n_fs, HD, HV), BF16),
            pltpu.VMEM((n_fs, HD, HV), BF16),
            pltpu.VMEM((n_fs, rows, HV), BF16),
            pltpu.VMEM((2, HALF, HEADS * HD), BF16),
            pltpu.VMEM((2, HALF, HEADS * HV), BF16),
            dma((2,)),
            dma((4,)),
            dma((n_sp,)),
            dma((4, 2)),
            dma((n_sp,)),
            dma((8,)),
            dma((n_sp,)),
            dma((HEADS,)),
            dma((4,)),
            dma((4,)),
            dma((4, 2)),
            dma((HEADS,)),
            dma((2,)),
            dma((2,)),
        ],
        compiler_params=pltpu.CompilerParams(
            collective_id=1, has_side_effects=True, vmem_limit_bytes=40 * 1024 * 1024
        ),
        name="mix",
    )(
        *made,
        init_state.reshape(n_fs, HD, HV),
        diff_lambda,
        mix_gain.reshape(1, -1),
        state_gain.reshape(1, -1),
        output_attend,
        output_linear,
    )
    return out[None]


def solution(mesh):
    heads = P(None, ("fs", "tp"), None)
    in_specs = (
        P(("grp", "fs"), "sp", None),
        P(),
        heads,
        heads,
        heads,
        heads,
        heads,
        heads,
        P(),
        P(),
        P(),
        P(("grp", "fs"), "sp", None),
        P(),
        P(),
        P(),
        P(),
        P(),
        P("grp", ("fs", "tp"), None, None),
        P(None, "tp"),
        P(None, "tp"),
    )
    out_specs = P(("grp", "fs"), "sp", "tp")
    return jax.shard_map(body, mesh=mesh, in_specs=in_specs, out_specs=out_specs, check_vma=False)
```

time: 284 us -> 132 us (0.46)
  waiting for transfers between devices: 122 us -> 0 us
  Pallas kernels: 0 us -> 115 us
  blocking collectives: 46.6 us -> 0 us
  local copies, waits for them, and re-layouts: 50.1 us -> 16.3 us
  matrix products: 18.8 us -> 0 us
  starting transfers between devices: 17.8 us -> 0 us
  between operations: 14 us -> 0.07 us
  loops' own time: 5.99 us -> 0 us
  other arithmetic: 5.69 us -> 0 us
    pallas_call x0 -> x2, Pallas kernels: none -> 115 us  [the longest x1 96.8 us: body(): pl.pallas_call(mix_kernel, out_shape=jax.ShapeDtypeStruct((rows, cols), B...]
    all_gather x2 -> x0, waiting for transfers between devices: 96.2 us -> none  [the longest x1 77.6 us: entering(): gathered = jax.tree.map(lambda a: lax.all_gather(a, axis), part)]
    all_gather x2 -> x0, blocking collectives: 46.6 us -> none  [the longest x1 43.5 us: entering(): gathered = jax.tree.map(lambda a: lax.all_gather(a, axis), part)]
    all_to_all x3 -> x0, waiting for transfers between devices: 25.3 us -> none  [the longest x1 17.5 us: sent_to_all(): return lax.all_to_all(copies, axis, split_axis=0, concat_axis=0, tiled=True)]
    dot_general x15 -> x0, matrix products: 18.8 us -> none  [the longest x1 5.96 us: body(): jnp.einsum('std,dp->stp', gather_directly(normed, 'fs', 0), packed, prefe...]
    all_to_all x3 -> x0, starting transfers between devices: 17.7 us -> none  [the longest x1 6.75 us: body(): lax.all_to_all(init_state, 'fs', split_axis=0, concat_axis=1, tiled=True)[0]]
    dynamic_slice x14 -> x0, local copies, waits for them, and re-layouts: 10.2 us -> none  [the longest x8 4.69 us: body(): lax.scan(one_step, carry, (jnp.arange(step_count, dtype=jnp.int32), key_s...]
    unnamed x63 -> x41, local copies, waits for them, and re-layouts: 22.9 us -> 16.3 us
  transfers between devices with their start and end apart: 5 -> 0, of which waited for: 4 -> 0; matrix products, arithmetic and copies ran while one was open for 17% -> 0% of each run, Pallas kernels for 0% -> 0%
where the time goes in v1:
time: 132 us; the launch traced here: 131 us
  Pallas kernels  115 us (87%)
  local copies, waits for them, and re-layouts  16.3 us (12%)
    pallas_call x1, Pallas kernels, body(): pl.pallas_call(mix_kernel, out_shape=jax.ShapeDtypeStruct((rows, cols), B...  96.8 us
    pallas_call x1, Pallas kernels, body(): pl.pallas_call(project_kernel, out_shape=[jax.ShapeDtypeStruct((n_fs, row...  17.9 us
    unnamed x41, local copies, waits for them, and re-layouts  16.3 us

profile of v1, /device:TPU:45, one launch (start us, length us, event | category | flops | bytes accessed | tf_op | source)
XLA Modules:
  0.0 131.1 jit_solution(15040503084114580523)
XLA Ops:
  0.0 0.0 copy-start
  0.0 0.0 copy-start.2
  0.0 1.4 %copy-done.2 = bf16[2048,1,256]{2,0,1:T(8,128)(2,1)S(1)} copy-done((bf16[2048,1,256]{2,0,1:T(8,128)(2,1)S(1)}, bf16[2048,1,256]{2,0,1:T(8,128)(2,1)}, u32[]{:S(2)}) %copy-start.2) | copy-done | bytes 1048600
  1.4 0.0 copy-start.3
  1.4 1.2 copy-done.3
  2.6 0.0 copy-start.4
  2.6 1.0 copy-done.4
  3.7 0.0 copy-start.5
  3.7 1.0 copy-done.5
  4.7 0.0 copy-start.6
  4.7 1.0 copy-done.6
  5.7 0.0 copy-start.7
  5.7 1.0 copy-done.7
  6.8 0.0 copy-start.8
  6.8 1.0 copy-done.8
  7.8 0.0 copy-start.10
  7.8 0.9 copy-done.10
  8.7 0.0 copy-start.11
  8.7 0.8 copy-done.11
  9.6 0.0 copy-start.12
  9.6 0.7 copy-done.12
  10.3 0.0 copy-start.13
  10.3 0.7 copy-done.13
  11.0 0.0 copy-start.14
  11.0 0.7 copy-done.14
  11.7 0.0 copy-start.15
  11.7 0.7 copy-done.15
  12.3 0.0 copy-start.17
  12.3 0.7 copy-done.17
  13.0 0.0 copy-start.16
  13.0 0.0 copy-start.18
  13.0 0.0 copy-start.19
  13.0 17.9 %project.1 = (bf16[4,128,256]{2,1,0:T(8,128)(2,1)S(1)}, bf16[4,128,128]{2,1,0:T(8,128)(2,1)S(1)}, bf16[4,128,128]{2,1,0:T(8,128)(2,1)S(1)}, f32[4,128,256]{2,1,0...) custom-call(bf16[128,2048]{1,0:T(8,128)(2,1)S(1)} %bitcast.20, f32[1,2048]{1,0:T(1,128)S(1)} %bitcast.29, ...), custom_call_target="tpu_custom_call" | custom-call | tf_op jit(solution)/shard_map/project/pallas_call | solution.py:657
  30.9 0.0 copy-done
  30.9 0.0 copy-done.16
  30.9 0.0 copy-done.18
  30.9 0.0 copy-done.19
  30.9 0.0 copy-start.1
  30.9 1.6 %copy-done.1 = bf16[1024,1024]{1,0:T(8,128)(2,1)S(1)} copy-done((bf16[1024,1024]{1,0:T(8,128)(2,1)S(1)}, bf16[1024,1024]{1,0:T(8,128)(2,1)}, u32[]{:S(2)}) %copy-start.1) | copy-done | bytes 2097176
  32.5 0.0 copy-start.9
  32.5 1.0 copy-done.9
  33.6 96.8 %mix.1 = bf16[128,1024]{1,0:T(8,128)(2,1)S(1)} custom-call(bf16[4,128,256]{2,1,0:T(8,128)(2,1)S(1)} %get-tuple-element.11.kv_ref, bf16[4,128,128]{2,1,0:T(8,128)(2,1)S(1)} %get-tuple-element.12.q_ref, bf16[4,128,128]{2,1,0:T(8,128)(2,1)S(1)} %get-tuple-element.13.qr_ref, f32[4,128,256]{2,1,0:T(8,128)S(1)} %get-tuple-element.14.inside_ref, ...), custom_call_target="tpu_custom_call" | custom-call | tf_op jit(solution)/shard_map/mix/pallas_call | solution.py:695
  130.3 0.7 copy.22
Async XLA Ops:
  0.0 30.9 %copy-start = (bf16[2048,1024]{1,0:T(8,128)(2,1)S(1)}, bf16[2048,1024]{1,0:T(8,128)(2,1)}, u32[]{:S(2)}) copy-start(bf16[2048,1024]{1,0:T(8,128)(2,1)} %wl_hbm.1) | copy-start | bytes 12582916
  0.0 1.4 %copy-start.2 = (bf16[2048,1,256]{2,0,1:T(8,128)(2,1)S(1)}, bf16[2048,1,256]{2,0,1:T(8,128)(2,1)}, u32[]{:S(2)}) copy-start(bf16[2048,1,256]{2,0,1:T(8,128)(2,1)} %param.27) | copy-start | bytes 3145732
  1.4 1.2 copy-start.3
  2.6 1.0 copy-start.4
  3.7 1.0 copy-start.5
  4.7 1.0 copy-start.6
  5.7 1.0 copy-start.7
  6.8 1.0 copy-start.8
  7.8 0.9 copy-start.10
  8.7 0.8 copy-start.11
  9.6 0.7 copy-start.12
  10.3 0.7 copy-start.13
  11.0 0.7 copy-start.14
  11.7 0.7 copy-start.15
  12.3 0.7 copy-start.17
  13.0 17.9 %copy-start.16 = (f32[256]{0:T(256)S(1)}, f32[256]{0:T(256)}, u32[]{:S(2)}) copy-start(f32[256]{0:T(256)} %param.36) | copy-start | bytes 3076
  13.0 17.9 %copy-start.18 = (f32[8]{0:T(128)S(1)}, f32[8]{0:T(128)}, u32[]{:S(2)}) copy-start(f32[8]{0:T(128)} %lam_ref.1) | copy-start | bytes 100
  13.0 17.9 %copy-start.19 = (f32[128]{0:T(128)S(1)}, f32[128]{0:T(128)}, u32[]{:S(2)}) copy-start(f32[128]{0:T(128)} %param.35) | copy-start | bytes 1540
  30.9 1.6 %copy-start.1 = (bf16[1024,1024]{1,0:T(8,128)(2,1)S(1)}, bf16[1024,1024]{1,0:T(8,128)(2,1)}, u32[]{:S(2)}) copy-start(bf16[1024,1024]{1,0:T(8,128)(2,1)} %wa_hbm.1) | copy-start | bytes 6291460
  32.5 1.0 copy-start.9

commit v2 on v1

v2 whole, which is shorter than its diff:
```python
import functools

import jax
import jax.numpy as jnp
from jax import lax
from jax.experimental import pallas as pl
from jax.experimental.pallas import tpu as pltpu
from jax.sharding import PartitionSpec as P

HEADS = 8
HALF = 64
HD = 128
HV = 256
BLK = 64
RANK = 32
EPS = 1e-06
TAU = 16.0
MESH = pl.DeviceIdType.MESH
F32 = jnp.float32
BF16 = jnp.bfloat16
NT = (((1,), (1,)), ((), ()))
TN = (((0,), (0,)), ((), ()))


def dot(a, b, dims=(((1,), (0,)), ((), ())), **kw):
    return lax.dot_general(a, b, dims, preferred_element_type=F32, **kw)


def iota(shape, dim):
    return lax.broadcasted_iota(jnp.int32, shape, dim)


def turned(row, n):
    return jnp.transpose(jnp.broadcast_to(row, (n, row.shape[-1])))


def unit_norm(x, gain):
    left = iota(x.shape, 1) < HALF
    sq = x * x
    a = jnp.sum(jnp.where(left, sq, 0.0), axis=1, keepdims=True)
    b = jnp.sum(jnp.where(left, 0.0, sq), axis=1, keepdims=True)
    mean = jnp.where(left, a, b) * (1.0 / HALF)
    return (x * lax.rsqrt(mean + EPS) * gain).astype(BF16)


def layer_kernel(
    tok_hbm,
    gain_hbm,
    wqa,
    wka,
    wva,
    wql,
    wkl,
    wvl,
    down_hbm,
    up_hbm,
    bias_hbm,
    retain_hbm,
    qgain_hbm,
    kgain_hbm,
    lam_ref,
    mix_gain_hbm,
    state_gain_hbm,
    init_hbm,
    wa_hbm,
    wl_hbm,
    out_ref,
    tok,
    gain_v,
    weights,
    down,
    up,
    bias_v,
    qgain_v,
    kgain_v,
    mix_gain,
    state_gain,
    init,
    wa,
    wl,
    gath,
    rets,
    kvs,
    qs,
    qr,
    inside,
    local,
    dec,
    kvbuf,
    qbuf,
    abuf,
    sin,
    sout,
    lbuf,
    fa,
    fl,
    in_sem,
    send,
    recv,
    r_send,
    r_recv,
    kv_send,
    kv_recv,
    q_send,
    q_recv,
    relay_send,
    a_send,
    a_recv,
    c_send,
    c_recv,
    l_send,
    l_recv,
    f_send,
    f_recv,
    up_sem,
    ready_sem,
):
    x = lax.axis_index("fs")
    t = lax.axis_index("tp")
    z = lax.axis_index("sp")
    n_sp = lax.axis_size("sp")
    n_fs = lax.axis_size("fs")
    n_work = 2 * n_fs
    right, left, far = lax.rem(x + 1, n_fs), lax.rem(x + n_fs - 1, n_fs), lax.rem(x + 2, n_fs)
    seqs = (x, left, far, right)
    order = (0, 1, 3, 2)
    head = x * 2 + t
    rows = tok.shape[0]
    partner = {"tp": 1 - t}
    first, last = z == 0, z == n_sp - 1
    worker = z < n_work
    w_seq = z // 2
    w_tp = lax.rem(z, 2)
    w_head = x * 2 + w_tp
    kv_core = lax.rem(z, 2)

    barrier = pltpu.get_barrier_semaphore()

    def tell(sem, dev):
        pl.semaphore_signal(sem, inc=1, device_id=dev, device_id_type=MESH)

    for peer in (right, left, far):
        for tt in range(2):
            tell(barrier, {"fs": peer, "tp": tt})
    tell(barrier, partner)
    pl.when(jnp.logical_not(first))(lambda: tell(barrier, {"sp": lax.rem(z + n_sp - 1, n_sp)}))
    pl.when(jnp.logical_not(last))(lambda: tell(barrier, {"sp": lax.rem(z + 1, n_sp)}))

    loads = []

    def load(src, dst):
        c = pltpu.make_async_copy(src, dst, in_sem.at[len(loads)])
        loads.append(c)
        c.start()

    load(tok_hbm, tok)
    load(gain_hbm, gain_v)
    load(retain_hbm, rets.at[0])
    at = 0
    for w in (wqa, wka, wva, wql, wkl, wvl):
        width = w.shape[1]
        load(w, weights.at[:, pl.ds(at, width)])
        at += width
    load(down_hbm, down)
    load(up_hbm, up)
    load(bias_hbm, bias_v)
    load(qgain_hbm, qgain_v)
    load(kgain_hbm, kgain_v)
    load(mix_gain_hbm, mix_gain)
    load(state_gain_hbm, state_gain)
    for slot in range(n_fs):
        load(init_hbm.at[seqs[slot]], init.at[slot])
    load(wa_hbm, wa)
    load(wl_hbm, wl)
    for c in loads[:3]:
        c.wait()
    gain = gain_v[...]

    def normalize(start):
        part = tok[pl.ds(start, 32), :].astype(F32)
        mean = jnp.mean(part * part, axis=1, keepdims=True)
        gath[0, pl.ds(start, 32), :] = (part * lax.rsqrt(mean + EPS) * gain).astype(BF16)

    lo = pl.multiple_of(t * 64, 64)
    hi = pl.multiple_of(t * 64 + 32, 32)
    other = pl.multiple_of((1 - t) * 64, 64)
    other_hi = pl.multiple_of((1 - t) * 64 + 32, 32)
    normalize(lo)
    normalize(hi)
    with jax.named_scope("bar"):
        pl.semaphore_wait(
            barrier,
            7 + jnp.logical_not(first).astype(jnp.int32) + jnp.logical_not(last).astype(jnp.int32),
        )

    def remote(i, slot_from, slot_to, start, peer):
        return pltpu.make_async_remote_copy(
            src_ref=gath.at[slot_from, pl.ds(start, 32), :],
            dst_ref=gath.at[slot_to, pl.ds(start, 32), :],
            send_sem=send.at[i],
            recv_sem=recv.at[i],
            device_id=peer,
            device_id_type=MESH,
        )

    to_right = {"fs": right}
    to_left = {"fs": left}
    r0 = remote(0, 0, 1, lo, to_right)
    l1 = remote(1, 0, 3, hi, to_left)
    r1 = remote(2, 0, 1, hi, to_right)
    l0 = remote(3, 0, 3, lo, to_left)
    for c in (r0, l1, r1, l0):
        c.start()
    small = []
    for i, (slot, peer) in enumerate(((1, right), (3, left), (2, far))):
        small.append(
            pltpu.make_async_remote_copy(
                src_ref=rets.at[0],
                dst_ref=rets.at[slot],
                send_sem=r_send.at[i],
                recv_sem=r_recv.at[i],
                device_id={"fs": peer},
                device_id_type=MESH,
            )
        )
    for c in small:
        c.start()

    with jax.named_scope("upw"):

        @pl.when(jnp.logical_not(first))
        def _():
            pl.semaphore_wait(up_sem, 1)

    pl.when(jnp.logical_not(last))(lambda: tell(up_sem, {"sp": lax.rem(z + 1, n_sp)}))

    @pl.when(worker)
    def _():
        def lower(zz, c):
            tell(ready_sem, {"sp": zz, "tp": 0})
            tell(ready_sem, {"sp": zz, "tp": 1})
            return c

        lax.fori_loop(0, z, lower, 0)

    normalize(other)
    normalize(other_hi)
    with jax.named_scope("wwait"):
        for c in loads[3:14]:
            c.wait()

    up_rows = up[...]
    pick = iota((RANK, RANK * HEADS), 1) == iota((RANK, RANK * HEADS), 0) * HEADS + head
    pick = jnp.where(pick, 1.0, 0.0).astype(BF16)
    bias = bias_v[pl.ds(head, 1), :]
    qg = qgain_v[...]
    qgain = jnp.concatenate([qg, qg], axis=1)
    kg = kgain_v[pl.ds(head, 1)][0]
    kgain = jnp.concatenate([kg[0:1], kg[1:2]], axis=1)
    rr, cc = iota((rows, rows), 0), iota((rows, rows), 1)
    same = (rr // BLK) == (cc // BLK)
    tri = jnp.where(same & (rr >= cc), 1.0, 0.0)
    second = iota((rows, HD), 0) >= BLK

    def finish(slot):
        act = gath[slot]
        got = dot(act, weights[...]).astype(BF16)
        low = dot(act, down[...], NT).astype(BF16)
        pre = dot(dot(low, pick).astype(BF16), up_rows) + bias
        log_sig = jnp.minimum(pre, 0.0) - jnp.log1p(jnp.exp(-jnp.abs(pre)))
        keep = jnp.sum(
            jnp.where(iota((HEADS, rows), 0) == head, rets[slot], 0.0), axis=0, keepdims=True
        )
        log_decay = log_sig * (1.0 / TAU) + turned(keep, HD)
        run = dot(tri, log_decay, precision=lax.Precision.HIGHEST)
        q_unit = unit_norm(got[:, 0:HD].astype(F32), qgain)
        k_unit = unit_norm(got[:, HD : 2 * HD].astype(F32), kgain)
        kvs[slot, :, 0:HD] = k_unit
        kvs[slot, :, HD : 2 * HD] = got[:, 2 * HD : 3 * HD]
        qs[slot] = (q_unit.astype(F32) * (HALF**-0.5)).astype(BF16)
        q_lin = got[:, 3 * HD : 4 * HD].astype(F32) * (HD**-0.5)
        k_lin = got[:, 4 * HD : 5 * HD].astype(F32)
        v_lin = got[:, 5 * HD :]
        mid = BLK // 2
        pivot = jnp.where(second, run[BLK + mid : BLK + mid + 1], run[mid : mid + 1])
        end0, end1 = run[BLK - 1 : BLK], run[2 * BLK - 1 : 2 * BLK]
        ends = jnp.where(second, end1, end0)
        scores = dot(
            (q_lin * jnp.exp(run - pivot)).astype(BF16),
            (k_lin * jnp.exp(pivot - run)).astype(BF16),
            NT,
        )
        q_here = q_lin * jnp.exp(run)
        k_left = k_lin * jnp.exp(ends - run)
        across = dot(q_here.astype(BF16), k_left.astype(BF16), NT)
        later = (rr >= BLK) & (cc < BLK)
        mixed = jnp.where(same & (rr >= cc), scores, jnp.where(later, across, 0.0))
        inside[slot] = dot(mixed.astype(BF16), v_lin)
        k_out = k_left * jnp.where(second, 1.0, jnp.exp(end1))
        local[slot] = dot(k_out.astype(BF16), v_lin, TN)
        qr[slot] = (q_here * jnp.where(second, jnp.exp(end0), 1.0)).astype(BF16)
        dec[slot] = turned(jnp.exp(end0 + end1), HD)

    finish(0)

    f_right = remote(4, 1, 2, lo, to_right)
    f_left = remote(5, 3, 2, hi, to_left)
    relays = {
        "r0": remote(6, 1, 1, lo, partner),
        "l1": remote(7, 3, 3, hi, partner),
        "r1": remote(8, 1, 1, hi, partner),
        "l0": remote(9, 3, 3, lo, partner),
        "f0": remote(10, 2, 2, lo, partner),
        "f1": remote(11, 2, 2, hi, partner),
    }
    with jax.named_scope("p_r0"):
        r0.wait_recv()
    f_right.start()
    relays["r0"].start()
    l1.wait_recv()
    f_left.start()
    relays["l1"].start()
    with jax.named_scope("p_r1"):
        r1.wait_recv()
    relays["r1"].start()
    l0.wait_recv()
    relays["l0"].start()
    for c in small:
        c.wait_recv()
    with jax.named_scope("p_rel1"):
        relays["r0"].wait_recv()
        relays["r1"].wait_recv()
    finish(1)
    with jax.named_scope("p_f"):
        f_right.wait_recv()
        relays["f0"].start()
        f_left.wait_recv()
        relays["f1"].start()
        relays["l1"].wait_recv()
        relays["l0"].wait_recv()
    finish(3)
    with jax.named_scope("p_relf"):
        relays["f0"].wait_recv()
        relays["f1"].wait_recv()
    finish(2)

    def kv_copy(slot, dst_z):
        return pltpu.make_async_remote_copy(
            src_ref=kvs.at[slot],
            dst_ref=kvbuf.at[z],
            send_sem=kv_send.at[slot],
            recv_sem=kv_recv.at[z],
            device_id={"sp": dst_z, "tp": kv_core},
            device_id_type=MESH,
        )

    def q_copy(slot, dst_z, dst_t):
        return pltpu.make_async_remote_copy(
            src_ref=qs.at[slot, pl.ds(dst_t * HALF, HALF), :],
            dst_ref=qbuf.at[z],
            send_sem=q_send.at[slot, dst_t],
            recv_sem=q_recv.at[z],
            device_id={"sp": dst_z, "tp": dst_t},
            device_id_type=MESH,
        )

    def spread(start):
        for slot in order:
            pz = 2 * seqs[slot] + t
            mine = (pz == z) & (kv_core == t)
            c = kv_copy(slot, pz)
            pl.when(jnp.logical_not(mine))(c.start if start else c.wait_send)
            if start:

                @pl.when(mine)
                def _():
                    kvbuf[z] = kvs[slot]

            for tt in range(2):
                mine_q = (pz == z) & (t == tt)
                c = q_copy(slot, pz, tt)
                pl.when(jnp.logical_not(mine_q))(c.start if start else c.wait_send)
                if start:

                    @pl.when(mine_q)
                    def _():
                        qbuf[z] = qs[slot, tt * HALF : (tt + 1) * HALF, :]

    n_piece = 2
    piece = HD // n_piece

    def chain_copy(slot, k):
        part = pl.ds(k * piece, piece)
        return pltpu.make_async_remote_copy(
            src_ref=sout.at[slot, part, :],
            dst_ref=sin.at[slot, part, :],
            send_sem=c_send.at[slot, k],
            recv_sem=c_recv.at[slot, k],
            device_id={"sp": lax.rem(z + 1, n_sp)},
            device_id_type=MESH,
        )

    def lin_copy(slot, tt):
        return pltpu.make_async_remote_copy(
            src_ref=lbuf.at[slot, pl.ds(tt * HALF, HALF), :],
            dst_ref=fl.at[tt, :, pl.ds(pl.multiple_of(head * HV, HV), HV)],
            send_sem=l_send.at[slot, tt],
            recv_sem=l_recv.at[head],
            device_id={"fs": seqs[slot], "tp": tt},
            device_id_type=MESH,
        )

    def passed_on(slot, k, value):
        part = slice(k * piece, (k + 1) * piece)
        d = dec[slot, part, :]
        d = jnp.concatenate([d, d], axis=1)
        sout[slot, part, :] = (value * d + local[slot, part, :]).astype(BF16)
        chain_copy(slot, k).start()

    def chain_start():
        for c in loads[16:20]:
            c.wait()
        for slot in order:
            sin[slot] = init[slot].astype(BF16)
            for k in range(n_piece):
                passed_on(slot, k, init[slot, k * piece : (k + 1) * piece, :])

    def chain():
        @pl.when(jnp.logical_not(first | last))
        def _():
            for slot in order:
                for k in range(n_piece):
                    with jax.named_scope("cwait"):
                        chain_copy(slot, k).wait_recv()
                    passed_on(slot, k, sin[slot, k * piece : (k + 1) * piece, :].astype(F32))

        for slot in order:

            @pl.when(last)
            def _():
                with jax.named_scope("cwait"):
                    for k in range(n_piece):
                        chain_copy(slot, k).wait_recv()

            raw = inside[slot] + dot(qr[slot], sin[slot])
            mean = jnp.mean(raw * raw, axis=1, keepdims=True)
            lin = (raw * lax.rsqrt(mean + EPS) * state_gain[...]).astype(BF16)
            lbuf[slot] = lin
            for tt in range(2):
                if slot:
                    lin_copy(slot, tt).start()
                else:
                    pl.when(t != tt)(lin_copy(slot, tt).start)

                    @pl.when(t == tt)
                    def _():
                        fl[tt, :, pl.ds(pl.multiple_of(head * HV, HV), HV)] = lin[
                            tt * HALF : (tt + 1) * HALF
                        ]

    def relay_copy(j):
        zz = t + 2 * j
        return pltpu.make_async_remote_copy(
            src_ref=kvbuf.at[zz],
            dst_ref=kvbuf.at[zz],
            send_sem=relay_send.at[j],
            recv_sem=kv_recv.at[zz],
            device_id=partner,
            device_id_type=MESH,
        )

    def kv_arrival(zz):
        return pltpu.make_async_remote_copy(
            src_ref=kvs.at[0],
            dst_ref=kvbuf.at[zz],
            send_sem=kv_send.at[0],
            recv_sem=kv_recv.at[zz],
            device_id=partner,
            device_id_type=MESH,
        )

    def q_arrival(zz):
        return pltpu.make_async_remote_copy(
            src_ref=qs.at[0, pl.ds(0, HALF), :],
            dst_ref=qbuf.at[zz],
            send_sem=q_send.at[0, 0],
            recv_sem=q_recv.at[zz],
            device_id=partner,
            device_id_type=MESH,
        )

    def a_copy(i):
        return pltpu.make_async_remote_copy(
            src_ref=abuf.at[i],
            dst_ref=fa.at[t, :, pl.ds(pl.multiple_of(w_head * HD, HD), HD)],
            send_sem=a_send.at[i],
            recv_sem=a_recv.at[w_head],
            device_id={"fs": w_seq, "sp": i},
            device_id_type=MESH,
        )

    def attend(g):
        lam = lam_ref[w_head]
        own = t == w_tp
        span = 512 * (g + 1)
        with jax.named_scope("kvwait"):
            for j in range(2 * g, 2 * g + 2):
                zz = t + 2 * j
                pl.when(jnp.logical_not(own & (zz == z)))(kv_arrival(zz).wait_recv)
                relay_copy(j).start()
        with jax.named_scope("qwait"):
            for i in range(4 * g, 4 * g + 4):
                pl.when(jnp.logical_not(own & (z == i)))(q_arrival(i).wait_recv)
        with jax.named_scope("rwait"):
            for j in range(2 * g, 2 * g + 2):
                kv_arrival((1 - t) + 2 * j).wait_recv()

        def one(i, c):
            qi = qbuf[i]
            lane = iota((HALF, HD), 1)
            zero = jnp.zeros_like(qi)
            q2 = jnp.concatenate(
                [jnp.where(lane < HALF, qi, zero), jnp.where(lane < HALF, zero, qi)], axis=0
            )
            n_old = 4 * g
            keys = kvbuf[n_old : n_old + 4, :, 0:HD].reshape(512, HD)
            vals = kvbuf[n_old : n_old + 4, :, HD:].reshape(512, HD)
            s = dot(q2, keys, NT)
            limit = (2 * i + t + 1) * BLK - span + 512
            s = jnp.where(iota(s.shape, 1) < limit, s, -jnp.inf)
            top = jnp.max(s, axis=1, keepdims=True)
            if g:
                old_keys = kvbuf[0:n_old, :, 0:HD].reshape(span - 512, HD)
                old_vals = kvbuf[0:n_old, :, HD:].reshape(span - 512, HD)
                s_old = dot(q2, old_keys, NT)
                top = jnp.maximum(top, jnp.max(s_old, axis=1, keepdims=True))
            p = jnp.exp(s - top)
            total = jnp.sum(p, axis=1, keepdims=True)
            acc = dot(p.astype(BF16), vals)
            if g:
                p_old = jnp.exp(s_old - top)
                total = total + jnp.sum(p_old, axis=1, keepdims=True)
                acc = acc + dot(p_old.astype(BF16), old_vals)
            acc = acc / total
            diff = acc[:HALF] - lam * acc[HALF:]
            mean = jnp.mean(diff * diff, axis=1, keepdims=True)
            res = (diff * lax.rsqrt(mean + EPS) * mix_gain[...]).astype(BF16)
            abuf[i] = res
            mine = (x == w_seq) & (z == i)
            pl.when(jnp.logical_not(mine))(a_copy(i).start)

            @pl.when(mine)
            def _():
                fa[t, :, pl.ds(pl.multiple_of(w_head * HD, HD), HD)] = res

            return c

        with jax.named_scope("attn"):
            lax.fori_loop(4 * g, 4 * g + 4, one, 0)

    for c in loads[14:16]:
        c.wait()
    pl.when(first)(chain_start)
    above = jnp.maximum(n_work - 1 - z, 0)
    with jax.named_scope("ready"):

        @pl.when(above > 0)
        def _():
            pl.semaphore_wait(ready_sem, 2 * above)

    with jax.named_scope("spread"):
        spread(True)

    chain_at = jnp.where(z < 4, 0, 1)

    def step(i, c):
        pl.when(i == chain_at)(chain)
        for g in range(4):
            pl.when(worker & (i == g))(functools.partial(attend, g))
        return c

    lax.fori_loop(0, 4, step, 0)

    @pl.when(jnp.logical_not(first))
    def _():
        for c in loads[16:20]:
            c.wait()

    def a_arrival(hh):
        return pltpu.make_async_remote_copy(
            src_ref=abuf.at[0],
            dst_ref=fa.at[t, :, pl.ds(hh * HD, HD)],
            send_sem=a_send.at[0],
            recv_sem=a_recv.at[hh],
            device_id=partner,
            device_id_type=MESH,
        )

    def l_arrival(hh):
        return pltpu.make_async_remote_copy(
            src_ref=lbuf.at[0, pl.ds(0, HALF), :],
            dst_ref=fl.at[t, :, pl.ds(hh * HV, HV)],
            send_sem=l_send.at[0, 0],
            recv_sem=l_recv.at[hh],
            device_id=partner,
            device_id_type=MESH,
        )

    def swap(buf, i):
        return pltpu.make_async_remote_copy(
            src_ref=buf.at[t],
            dst_ref=buf.at[t],
            send_sem=f_send.at[i],
            recv_sem=f_recv.at[i],
            device_id=partner,
            device_id_type=MESH,
        )

    for c in loads[20:]:
        c.wait()
    with jax.named_scope("await"):
        for hh in range(HEADS):
            from_me = (x == hh // 2) & (z == 2 * x + hh % 2)
            pl.when(jnp.logical_not(from_me))(a_arrival(hh).wait_recv)
    swap(fa, 0).start()
    with jax.named_scope("lwait"):
        for hh in range(HEADS):
            pl.when(head != hh)(l_arrival(hh).wait_recv)
    swap(fl, 1).start()
    swap(fa, 0).wait_recv()
    acc = dot(fa[...].reshape(2 * HALF, HEADS * HD), wa[...])
    with jax.named_scope("lswap"):
        swap(fl, 1).wait_recv()
    acc = acc + dot(fl[...].reshape(2 * HALF, HEADS * HV), wl[...])
    out_ref[...] = acc.astype(BF16)

    with jax.named_scope("drain"):
        swap(fa, 0).wait_send()
        swap(fl, 1).wait_send()
        for c in (r0, l1, r1, l0, f_right, f_left, *relays.values(), *small):
            c.wait_send()
        spread(False)
        for slot in order:
            for k in range(n_piece):
                pl.when(jnp.logical_not(last))(chain_copy(slot, k).wait_send)
            for tt in range(2):
                if slot:
                    lin_copy(slot, tt).wait_send()
                else:
                    pl.when(t != tt)(lin_copy(slot, tt).wait_send)

        @pl.when(worker)
        def _():
            for j in range(n_sp // 2):
                relay_copy(j).wait_send()

            def done(i, c):
                mine = (x == w_seq) & (z == i)
                pl.when(jnp.logical_not(mine))(a_copy(i).wait_send)
                return c

            lax.fori_loop(0, n_sp, done, 0)


def body(
    tokens,
    norm_gain,
    query_attend,
    key_attend,
    value_attend,
    query_linear,
    key_linear,
    value_linear,
    decay_down,
    decay_up,
    decay_bias,
    log_retain,
    query_gain,
    key_gain,
    diff_lambda,
    mix_gain,
    state_gain,
    init_state,
    output_attend,
    output_linear,
):
    rows, width = tokens.shape[1:]
    n_fs = lax.axis_size("fs")
    n_sp = lax.axis_size("sp")
    cols = output_attend.shape[1]
    flat = [
        w.reshape(w.shape[0], -1)
        for w in (query_attend, key_attend, value_attend, query_linear, key_linear, value_linear)
    ]
    total = sum(w.shape[1] for w in flat)
    vmem = pl.BlockSpec(memory_space=pltpu.VMEM)
    smem = pl.BlockSpec(memory_space=pltpu.SMEM)
    hbm = pl.BlockSpec(memory_space=pl.ANY)
    dma = pltpu.SemaphoreType.DMA
    V = pltpu.VMEM

    out = pl.pallas_call(
        layer_kernel,
        out_shape=jax.ShapeDtypeStruct((rows, cols), BF16),
        in_specs=[hbm] * 14 + [smem] + [hbm] * 5,
        out_specs=vmem,
        scratch_shapes=[
            V((rows, width), BF16),
            V((1, width), F32),
            V((width, total), BF16),
            V((RANK, width), BF16),
            V((RANK * HEADS, HD), BF16),
            V((HEADS, HD), F32),
            V((1, HALF), F32),
            V((HEADS, 2, HALF), F32),
            V((1, HD), F32),
            V((1, HV), F32),
            V((n_fs, HD, HV), F32),
            V(output_attend.shape, BF16),
            V(output_linear.shape, BF16),
            V((n_fs, rows, width), BF16),
            V((n_fs, HEADS, rows), F32),
            V((n_fs, rows, 2 * HD), BF16),
            V((n_fs, rows, HD), BF16),
            V((n_fs, rows, HD), BF16),
            V((n_fs, rows, HV), F32),
            V((n_fs, HD, HV), F32),
            V((n_fs, HD, HD), F32),
            V((n_sp, rows, 2 * HD), BF16),
            V((n_sp, HALF, HD), BF16),
            V((n_sp, HALF, HD), BF16),
            V((n_fs, HD, HV), BF16),
            V((n_fs, HD, HV), BF16),
            V((n_fs, rows, HV), BF16),
            V((2, HALF, HEADS * HD), BF16),
            V((2, HALF, HEADS * HV), BF16),
            dma((22,)),
            dma((12,)),
            dma((12,)),
            dma((3,)),
            dma((3,)),
            dma((n_fs,)),
            dma((n_sp,)),
            dma((n_fs, 2)),
            dma((n_sp,)),
            dma((n_sp // 2,)),
            dma((n_sp,)),
            dma((HEADS,)),
            dma((n_fs, 2)),
            dma((n_fs, 2)),
            dma((n_fs, 2)),
            dma((HEADS,)),
            dma((2,)),
            dma((2,)),
            pltpu.SemaphoreType.REGULAR,
            pltpu.SemaphoreType.REGULAR,
        ],
        compiler_params=pltpu.CompilerParams(
            collective_id=0, has_side_effects=True, vmem_limit_bytes=67043328
        ),
        name="layer",
    )(
        tokens[0],
        norm_gain.reshape(1, -1),
        *flat,
        decay_down.T,
        decay_up.reshape(-1, HD),
        decay_bias,
        log_retain[0].T,
        query_gain.reshape(1, -1),
        key_gain,
        diff_lambda,
        mix_gain.reshape(1, -1),
        state_gain.reshape(1, -1),
        init_state.reshape(n_fs, HD, HV),
        output_attend,
        output_linear,
    )
    return out[None]


def solution(mesh):
    heads = P(None, ("fs", "tp"), None)
    in_specs = (
        P(("grp", "fs"), "sp", None),
        P(),
        heads,
        heads,
        heads,
        heads,
        heads,
        heads,
        P(),
        P(),
        P(),
        P(("grp", "fs"), "sp", None),
        P(),
        P(),
        P(),
        P(),
        P(),
        P("grp", ("fs", "tp"), None, None),
        P(None, "tp"),
        P(None, "tp"),
    )
    out_specs = P(("grp", "fs"), "sp", "tp")
    return jax.shard_map(body, mesh=mesh, in_specs=in_specs, out_specs=out_specs, check_vma=False)
```

time: 132 us -> 97.3 us (0.74)
  the two profiles are of different devices: /device:TPU:45 before, /device:TPU:1959 now
where the time goes in v2:
time: 97.3 us; the launch traced here: 97.2 us
  Pallas kernels  95.5 us (98%)
  local copies, waits for them, and re-layouts  1.67 us (2%)
    pallas_call x1, Pallas kernels, body(): pl.pallas_call(layer_kernel, out_shape=jax.ShapeDtypeStruct((rows, cols),...  95.5 us

profile of v2, /device:TPU:1959, one launch (start us, length us, event | category | flops | bytes accessed | tf_op | source)
XLA Modules:
  0.0 97.2 jit_solution(9433935676542555842)
XLA Ops:
  0.0 95.5 %layer.1 = bf16[128,1024]{1,0:T(8,128)(2,1)} custom-call(bf16[128,2048]{1,0:T(8,128)(2,1)} %bitcast.20, f32[1,2048]{1,0:T(1,128)} %bitcast.29, bf16[2048,128]{1,0:T(8,128)(2,1)} %bitcast.21, bf16[2048,128]{1,0:T(8,128)(2,1)} %bitcast.22, bf16[2048,128]{1,0:T(8,128)(2,1)} %bitcast.23, bf16[2048,128]{1,0:T(8,128)(2,1)} %bitcast.24, ...), custom_call_target="tpu_custom_call" | custom-call | tf_op jit(solution)/shard_map/layer/pallas_call | solution.py:702
  95.5 1.7 %copy.22 = bf16[1,128,1024]{2,1,0:T(8,128)(2,1)} copy(bf16[1,128,1024]{2,1,0:T(8,128)(2,1)} %bitcast.18) | data formatting | bytes 524288
